TPU v7x, 32 devices: a whole 2x2x4 slice. The times are simulated.
32 devices in a mesh: st: 8 (over z, x), tp: 4 (over y, core).
Axes of the slice: x: 2, y: 2, z: 4, core: 2. Of those that a mesh axis runs over, the one named last changes fastest.
Arguments:
- tokens: bfloat16 [4096, 2048], P('st'), may hold values from -6 to 6
- mix_query: bfloat16 [2048, 1024], P(None, 'tp'), may hold values from -0.125 to 0.125
- mix_key: bfloat16 [2048, 1024], P(None, 'tp'), may hold values from -0.125 to 0.125
- mix_value: bfloat16 [2048, 1024], P(None, 'tp'), may hold values from -0.125 to 0.125
- decay_lower_map: bfloat16 [2048, 64], replicated, may hold values from -0.125 to 0.125
- decay_upper_map: bfloat16 [64, 1024], P(None, 'tp'), may hold values from -1 to 1
- decay_base: float32 [1024], P('tp'), may hold values from -7.5 to -2.5
- decay_shift: float32 [4096, 16], P('st', 'tp'), may hold values from -3.8 to 9.8
- rate_lower_map: bfloat16 [2048, 64], replicated, may hold values from -0.125 to 0.125
- rate_upper_map: bfloat16 [64, 1024], P(None, 'tp'), may hold values from -0.75 to 0.75
- norm_gain: float32 [1024], P('tp'), may hold values from 0.1 to 1.9
- mix_out: bfloat16 [1024, 2048], P(None, 'tp'), may hold values from -0.1875 to 0.1875
- cross_query: bfloat16 [2048, 2048], P(None, 'tp'), may hold values from -0.125 to 0.125
- score_gain: float32 [2048], P('tp'), may hold values from 0.1 to 1.9
- passage_key: bfloat16 [2048, 2048], P(None, 'tp'), may hold values from -0.125 to 0.125
- passage_value: bfloat16 [2048, 2048], P(None, 'tp'), may hold values from -0.125 to 0.125
- cross_out: bfloat16 [2048, 2048], P(None, 'tp'), may hold values from -0.5 to 0.5
- gate_down: bfloat16 [2048, 128], replicated, may hold values from -0.125 to 0.125
- gate_up: bfloat16 [128, 2048], P(None, 'tp'), may hold values from -0.5 to 0.5
- store: bfloat16 [96, 96, 2048], P('st'), may hold values from -6 to 6
- passage_ids: int32 [64, 4], P('st'), may hold values from 0 to 95, as said below
Outputs:
- mixed: bfloat16 [4096, 2048], P('st', 'tp')
Inputs may be any that keep to these rules, and one draw needn't show every extreme that they name: `passage_ids`: among the 32 passages named by the rows of one sequence, at most 4 are held by one index of st (passage p by index p // 12); in every draw exactly 4 are held by the index before the sequence's own.
All inputs are finite; a program needn't handle non-finite values.
Results may differ from a plain program's by a relative error of at most 0.0075.
Values may be sent and summed in bfloat16 or wider, within the bound.
A program may use at most 128 MiB of HBM per device.

v0:
```python
import jax
import jax.numpy as jnp
from jax import lax
from jax.sharding import PartitionSpec as P

XHEAD = 256
QBLOCK = 64
MBLOCK = 64


FLOAT32 = jnp.float32
BFLOAT = jnp.bfloat16
PRECISE = lax.Precision.HIGHEST


def rounded(values):
    return lax.optimization_barrier(values.astype(BFLOAT)).astype(FLOAT32)


def head_norm(values, head_size):
    shaped = values.reshape(values.shape[:-1] + (values.shape[-1] // head_size, head_size))
    scaled = shaped * lax.rsqrt(jnp.mean(shaped * shaped, axis=-1, keepdims=True) + 1e-06)
    return scaled.reshape(values.shape)


def pair_dots(left, right):
    return jnp.einsum("hsc,htc->hst", left, right, precision=PRECISE)


def apply_mat(matrix, vectors):
    return jnp.einsum("hst,htc->hsc", matrix, vectors, precision=PRECISE)


def block_step(state, inputs):
    query_vec, key_vec, value_vec, minus_key, rate_key, log_fade = inputs
    length = query_vec.shape[1]
    cumul_log = jnp.cumsum(log_fade, axis=1)
    before = cumul_log - log_fade
    block_end = cumul_log[:, -1:, :]
    row_idx = lax.broadcasted_iota(jnp.int32, (length, length), 0)
    col_idx = lax.broadcasted_iota(jnp.int32, (length, length), 1)
    strict = (col_idx < row_idx).astype(FLOAT32)
    upto_mask = (col_idx <= row_idx).astype(FLOAT32)
    minus_scaled = minus_key * jnp.exp(before)
    query_scaled = query_vec * jnp.exp(cumul_log)
    key_inverse = key_vec * jnp.exp(-cumul_log)
    rate_inverse = rate_key * jnp.exp(-cumul_log)
    key_pull = pair_dots(minus_scaled, key_inverse) * strict
    rate_pull = pair_dots(minus_scaled, rate_inverse) * strict
    key_read = pair_dots(query_scaled, key_inverse) * upto_mask
    rate_read = pair_dots(query_scaled, rate_inverse) * upto_mask
    solved = jnp.einsum("hsj,hij->hsi", minus_scaled, state, precision=PRECISE) + apply_mat(
        key_pull, value_vec
    )
    power_mat = rate_pull
    for repeat_idx in range((length - 1).bit_length()):
        solved = solved + apply_mat(power_mat, solved)
        power_mat = jnp.einsum("hst,htu->hsu", power_mat, power_mat, precision=PRECISE)
    outputs = (
        jnp.einsum("hsj,hij->hsi", query_scaled, state, precision=PRECISE)
        + apply_mat(key_read, value_vec)
        + apply_mat(rate_read, solved)
    )
    fade_out = jnp.exp(block_end - cumul_log)
    state = (
        state * jnp.exp(block_end)
        + jnp.einsum("hsi,hsj->hij", value_vec, key_vec * fade_out, precision=PRECISE)
        + jnp.einsum("hsi,hsj->hij", solved, rate_key * fade_out, precision=PRECISE)
    )
    return (state, outputs)


def mixer(
    tokens,
    mix_query,
    mix_key,
    mix_value,
    decay_lower_map,
    decay_upper_map,
    decay_base,
    decay_shift,
    rate_lower_map,
    rate_upper_map,
    norm_gain,
):
    tok_rows = tokens.shape[0]
    head_count = decay_shift.shape[1]
    mix_width = mix_query.shape[1]
    head_size = mix_width // head_count

    def project(weight):
        return rounded(jnp.dot(tokens, weight, preferred_element_type=FLOAT32))

    query_vec = project(mix_query)
    key_vec = project(mix_key)
    value_vec = project(mix_value)
    decay_low = jnp.tanh(jnp.dot(tokens, decay_lower_map, preferred_element_type=FLOAT32)).astype(
        BFLOAT
    )
    decay_pre = (
        decay_base
        + jnp.dot(decay_low, decay_upper_map, preferred_element_type=FLOAT32)
        + jnp.repeat(decay_shift, head_size, axis=1)
    )
    log_fade = -jnp.exp(-jax.nn.softplus(-decay_pre) - 0.5)
    rate_low = jnp.dot(tokens, rate_lower_map, preferred_element_type=FLOAT32).astype(BFLOAT)
    rate_gate = jax.nn.sigmoid(jnp.dot(rate_low, rate_upper_map, preferred_element_type=FLOAT32))

    def to_blocks(values):
        shaped = values.reshape(tok_rows // MBLOCK, MBLOCK, head_count, head_size)
        return shaped.transpose(0, 2, 1, 3)

    keyed = key_vec.reshape(tok_rows, head_count, head_size)
    unit_key = keyed * lax.rsqrt(jnp.sum(keyed * keyed, axis=-1, keepdims=True) + 1e-06)
    rate_key = unit_key * rate_gate.reshape(tok_rows, head_count, head_size)
    block_in = (
        to_blocks(query_vec),
        to_blocks(key_vec),
        to_blocks(value_vec),
        to_blocks(-unit_key),
        to_blocks(rate_key),
        to_blocks(log_fade),
    )
    state_zero = jnp.zeros((head_count, head_size, head_size), FLOAT32)
    _, head_out = lax.scan(block_step, state_zero, block_in)
    head_out = head_out.transpose(0, 2, 1, 3).reshape(tok_rows, head_count, head_size)
    centred = head_out - jnp.mean(head_out, axis=-1, keepdims=True)
    spread = jnp.mean(centred * centred, axis=-1, keepdims=True)
    normed = (centred * lax.rsqrt(spread + 0.00064)).reshape(tok_rows, mix_width)
    return (normed * norm_gain).astype(BFLOAT)


def local(
    tokens,
    mix_query,
    mix_key,
    mix_value,
    decay_lower_map,
    decay_upper_map,
    decay_base,
    decay_shift,
    rate_lower_map,
    rate_upper_map,
    norm_gain,
    mix_out,
    cross_query,
    score_gain,
    passage_key,
    passage_value,
    cross_out,
    gate_down,
    gate_up,
    store,
    passage_ids,
):
    mixer_heads = mixer(
        tokens,
        mix_query,
        mix_key,
        mix_value,
        decay_lower_map,
        decay_upper_map,
        decay_base,
        decay_shift,
        rate_lower_map,
        rate_upper_map,
        norm_gain,
    )
    tok_rows = tokens.shape[0]
    model_width = tokens.shape[1]
    owner_count = lax.axis_size("st")
    pass_dev = store.shape[0]
    passage_len = store.shape[1]
    cross_width = cross_query.shape[1]
    head_count = cross_width // XHEAD
    flat_ids = passage_ids.reshape(-1)
    slot_count = flat_ids.shape[0]
    capacity = max(2, -(-slot_count // owner_count))
    owner_of = flat_ids // pass_dev
    local_idx = flat_ids % pass_dev
    slot_order = jnp.arange(slot_count)
    earlier_same = (owner_of[:, None] == owner_of[None, :]) & (
        slot_order[None, :] < slot_order[:, None]
    )
    slot_rank = jnp.sum(earlier_same.astype(jnp.int32), axis=1)
    to_owner = owner_of[:, None] == jnp.arange(owner_count)[None, :]
    to_slot = slot_rank[:, None] == jnp.arange(capacity)[None, :]
    wanted = jnp.sum(
        jnp.where(to_owner[:, :, None] & to_slot[:, None, :], local_idx[:, None, None] + 1, 0),
        axis=0,
    )
    asked = lax.all_to_all(wanted, "st", split_axis=0, concat_axis=0, tiled=True)
    served = jnp.maximum(asked.reshape(-1) - 1, 0)
    where_from = owner_of * capacity + slot_rank
    row_share = passage_len // lax.axis_size("tp")
    own_rows = lax.dynamic_slice_in_dim(store, lax.axis_index("tp") * row_share, row_share, 1)
    outgoing = own_rows[served].reshape(owner_count, capacity, row_share, model_width)
    incoming = lax.all_to_all(outgoing, "st", split_axis=0, concat_axis=0, tiled=True)
    picked = incoming.reshape(owner_count * capacity, row_share, model_width)[where_from]
    piece = lax.all_gather(picked, "tp", axis=1, tiled=True)
    flat_rows = piece.reshape(-1, model_width)
    keyed = head_norm(
        jnp.dot(flat_rows, passage_key, preferred_element_type=FLOAT32), XHEAD
    ).astype(BFLOAT)
    valued = jnp.dot(flat_rows, passage_value, preferred_element_type=FLOAT32).astype(BFLOAT)
    joined = jnp.concatenate([keyed, valued], axis=-1)
    projected = joined.reshape(piece.shape[0], piece.shape[1], 2 * cross_width)
    block_count = tok_rows // QBLOCK
    queries = (
        head_norm(jnp.dot(tokens, cross_query, preferred_element_type=FLOAT32), XHEAD) * score_gain
    )
    queries = queries.astype(BFLOAT).reshape(block_count, QBLOCK, head_count, XHEAD)
    block_keys = projected[:, :, :cross_width].reshape(block_count, -1, head_count, XHEAD)
    block_values = projected[:, :, cross_width:].reshape(block_count, -1, head_count, XHEAD)
    scores = jnp.einsum(
        "bqhd,bkhd->bhqk", queries, block_keys, preferred_element_type=FLOAT32
    ) * XHEAD ** (-0.5)
    expon = jnp.exp(scores)
    weights = (expon / jnp.sum(expon, axis=-1, keepdims=True)).astype(BFLOAT)
    attended = jnp.einsum("bhqk,bkhd->bqhd", weights, block_values, preferred_element_type=FLOAT32)
    attended = attended.astype(BFLOAT).reshape(tok_rows, cross_width)
    shard_total = lax.axis_size("tp")
    out_cols = mix_out.shape[1]
    mix_rows = mix_out.reshape(shard_total, -1, out_cols)
    cross_rows = cross_out.reshape(shard_total, -1, out_cols)
    mixer_part = jnp.einsum(
        "ntc,ncd->td",
        lax.all_gather(mixer_heads[None], "tp", axis=0, tiled=True),
        mix_rows,
        preferred_element_type=FLOAT32,
    )
    cross_part = jnp.einsum(
        "ntc,ncd->td",
        lax.all_gather(attended[None], "tp", axis=0, tiled=True),
        cross_rows,
        preferred_element_type=FLOAT32,
    )
    gate_low = jnp.dot(tokens, gate_down, preferred_element_type=FLOAT32).astype(BFLOAT)
    gate_open = jax.nn.sigmoid(jnp.dot(gate_low, gate_up, preferred_element_type=FLOAT32))
    return (mixer_part + gate_open * cross_part).astype(BFLOAT)


def solution(mesh):
    placed = (
        P("st", None),
        P(None, "tp"),
        P(None, "tp"),
        P(None, "tp"),
        P(),
        P(None, "tp"),
        P("tp"),
        P("st", "tp"),
        P(),
        P(None, "tp"),
        P("tp"),
        P(None, "tp"),
        P(None, "tp"),
        P("tp"),
        P(None, "tp"),
        P(None, "tp"),
        P(None, "tp"),
        P(),
        P(None, "tp"),
        P("st", None, None),
        P("st", None),
    )
    return jax.shard_map(
        local, mesh=mesh, in_specs=placed, out_specs=P("st", "tp"), check_vma=False
    )
```

profile of v0, /device:TPU:0, one launch (start us, length us, event | category | flops | bytes accessed | tf_op | source)
XLA Modules:
  0.0 410.4 jit_solution(7020253587191063117)
XLA Ops:
  9.6 7.3 %all-to-all-start = ((s32[8,1,4]{2,1,0:T(1,128)}), s32[8,1,4]{2,1,0:T(1,128)S(1)}, u32[]{:S(2)}, u32[]{:S(2)}) async-start(s32[8,1,4]{2,1,0:T(1,128)} %copy.148), calls=%async_computation | async-start | bytes 8192 | tf_op jit(solution)/shard_map/all_to_all | solution.py:192
  16.9 1.3 constant_dynamic-slice_fusion
  18.3 5.1 %all-to-all-done = s32[8,1,4]{2,1,0:T(1,128)S(1)} async-done(((s32[8,1,4]{2,1,0:T(1,128)}), s32[8,1,4]{2,1,0:T(1,128)S(1)}, u32[]{:S(2)}, u32[]{:S(2)}) %all-to-all-start) | async-done | bytes 160 | tf_op jit(solution)/shard_map/all_to_all | solution.py:192
  23.4 2.4 gather_fusion
  25.9 4.4 %all-to-all-start.1 = ((bf16[8,4,24,2048]{3,2,1,0:T(8,128)(2,1)}), bf16[8,4,24,2048]{3,2,1,0:T(8,128)(2,1)}, u32[]{:S(2)}, u32[]{:S(2)}) async-start(bf16[8,4,24,2048]{3,2,1,0:T(8,128)(2,1)} %bitcast.271), calls=%async_computation.1 | async-start | bytes 6291456 | tf_op jit(solution)/shard_map/all_to_all | solution.py:198
  30.7 69.2 %all-to-all-done.1 = bf16[8,4,24,2048]{3,2,1,0:T(8,128)(2,1)} async-done(((bf16[8,4,24,2048]{3,2,1,0:T(8,128)(2,1)}), bf16[8,4,24,2048]{3,2,1,0:T(8,128)(2,1)}, u32[]{:S(2)}, u32[]{:S(2)}) %all-to-all-start.1) | async-done | bytes 3145760 | tf_op jit(solution)/shard_map/all_to_all | solution.py:198
  99.9 4.3 %gather_fusion.1 = bf16[32,24,2048]{2,1,0:T(8,128)(2,1)} fusion(bf16[32,24,2048]{2,1,0:T(8,128)(2,1)} %bitcast.15, s32[1024]{0:T(1024)S(1)} %pad_clamp_fusion), kind=kCustom, calls=%fused_computation.1 | custom fusion | bytes 6291584 | tf_op jit(solution)/shard_map/gather | solution.py:199
  104.3 4.0 copy.161
  108.3 4.2 %bitcast_reduce_fusion = (f32[512,2]{0,1:T(2,128)S(1)}, f32[512,512]{0,1:T(8,128)S(1)}) fusion(bf16[512,2048]{1,0:T(8,128)(2,1)} %param.23, bf16[2048,512]{1,0:T(8,128)(2,1)} %param.35), kind=kOutput, calls=%fused_computation.101 | convolution fusion | flops 1074265088 | bytes 5246976 | tf_op jit(solution)/shard_map/dot_general | solution.py:210
  112.7 1.5 reshape.416
  114.2 2.9 convolution_convert_fusion.2
  117.2 1.5 reshape.380
  119.1 2.7 fusion.52
  121.8 1.4 reshape.381
  123.5 2.9 fusion.65
  126.4 1.5 reshape.378
  127.9 2.6 convolution_convert_fusion.1
  130.5 1.4 reshape.394
  131.9 2.6 convolution_convert_fusion.3
  134.9 1.3 copy.133
  136.3 3.0 copy_bitcast_fusion
  139.3 2.1 fusion.59
  141.4 44.1 %all-gather.9.cloned.1.call-done = bf16[32,96,2048]{2,1,0:T(8,128)(2,1)} async-done(((bf16[32,24,2048]{2,1,0:T(8,128)(2,1)}), bf16[32,96,2048]{2,1,0:T(8,128)(2,1)}) %all-gather.9.cloned.1.call-update) | async-done | bytes 12582928 | tf_op jit(solution)/shard_map/all_gather | solution.py:200
  185.5 10.0 %multiply_reduce_fusion = (f32[3072,2]{0,1:T(2,128)S(1)}, f32[3072,2,256]{0,2,1:T(8,128)S(1)}) fusion(bf16[3072,2048,1]{1,0,2:T(8,128)(2,1)} %bitcast.282, bf16[2,256,2048]{2,1,0:T(8,128)(2,1)} %bitcast.276), kind=kOutput, calls=%fused_computation.63 | convolution fusion | flops 6445590528 | bytes 20996096 | tf_op jit(solution)/shard_map/dot_general | solution.py:203
  196.4 11.2 %convolution_convert_fusion = bf16[3072,512]{0,1:T(8,128)(2,1)} fusion(bf16[3072,2048]{1,0:T(8,128)(2,1)} %bitcast.283, bf16[2048,512]{1,0:T(8,128)(2,1)S(1)} %copy-done), kind=kOutput, calls=%fused_computation.64 | convolution fusion | flops 6444023808 | bytes 17825792 | tf_op jit(solution)/shard_map/dot_general | solution.py:205
  207.5 5.0 %pad_maximum_fusion = bf16[3072,1024]{0,1:T(8,128)(2,1)} fusion(bf16[3072,512]{0,1:T(8,128)(2,1)} %convolution_convert_fusion, bf16[3072,512]{0,1:T(8,128)(2,1)S(1)} %bitcast.272), kind=kLoop, calls=%fused_computation.61 | loop fusion | flops 12582912 | bytes 12582912 | tf_op jit(solution)/shard_map/concatenate | solution.py:206
  212.5 8.6 %copy.152 = bf16[3072,1024]{1,0:T(8,128)(2,1)} copy(bf16[3072,1024]{0,1:T(8,128)(2,1)} %pad_maximum_fusion) | data formatting | bytes 12582912 | tf_op jit(solution)/shard_map/concatenate | solution.py:206
  221.1 6.2 %fusion.76 = (bf16[32,96,512]{2,1,0:T(8,128)(2,1)}, bf16[32,96,512]{2,1,0:T(8,128)(2,1)}) fusion(bf16[32,96,1024]{2,1,0:T(8,128)(2,1)} %bitcast.270), kind=kLoop, calls=%fused_computation.152 | loop fusion | bytes 12582912 | tf_op jit(solution)/shard_map/slice | solution.py:213
  227.3 5.5 %reshape.391 = bf16[8,384,2,256]{3,2,1,0:T(2,128)(2,1)} reshape(bf16[32,96,512]{2,1,0:T(8,128)(2,1)} %get-tuple-element.105) | data formatting | bytes 6291456 | tf_op jit(solution)/shard_map/reshape | solution.py:213
  232.9 5.6 %reshape.389 = bf16[8,384,2,256]{3,2,1,0:T(2,128)(2,1)} reshape(bf16[32,96,512]{2,1,0:T(8,128)(2,1)} %get-tuple-element.106) | data formatting | bytes 6291456 | tf_op jit(solution)/shard_map/reshape | solution.py:214
  238.5 4.1 %multiply_exponential_fusion = f32[8,2,64,384]{3,2,1,0:T(8,128)} fusion(bf16[8,384,2,256]{3,2,1,0:T(2,128)(2,1)} %reshape.391, bf16[8,64,2,256]{1,0,3,2:T(8,128)(2,1)S(1)} %copy-done.5), kind=kOutput, calls=%fused_computation.70 | convolution fusion | flops 201719808 | bytes 5242880 | tf_op jit(solution)/shard_map/bqhd,bkhd->bhqk/dot_general | solution.py:215
  242.6 4.4 %fusion.47 = bf16[8,64,2,256]{3,1,2,0:T(8,128)(2,1)} fusion(bf16[8,384,2,256]{3,2,1,0:T(2,128)(2,1)} %reshape.389, f32[8,2,64,384]{3,2,1,0:T(8,128)} %multiply_exponential_fusion), kind=kOutput, calls=%fused_computation.82 | convolution fusion | flops 202376576 | bytes 5242880 | tf_op jit(solution)/shard_map/bhqk,bkhd->bqhd/dot_general | solution.py:220
  247.0 1.7 copy.157
  249.9 131.2 %while.13 = (s32[]{:T(128)}, f32[4,64,64]{2,1,0:T(8,128)S(1)}, f32[8,4,64,64]{3,2,1,0:T(8,128)S(1)}, f32[8,4,64,64]{3,2,1,0:T(8,128)S(1)}, f32[8,4,64,64]{2,3,1,...) while((s32[]{:T(128)}, f32[4,64,64]{2,1,0:T(8,128)S(1)}, ...), condition=%wide.region_3.4_spmd.clone, body=%wide.region_1.3_spmd.clone.sunk | while | flops 278528000 | bytes 7845517 | solution.py:125
  251.5 1.3 convolution_multiply_fusion.8
  254.1 1.3 convolution_multiply_fusion.9
  267.9 1.3 convolution_multiply_fusion.8
  270.5 1.3 convolution_multiply_fusion.9
  284.3 1.3 convolution_multiply_fusion.8
  286.9 1.3 convolution_multiply_fusion.9
  319.6 1.3 convolution_multiply_fusion.9
  336.0 1.3 convolution_multiply_fusion.9
  349.7 1.3 convolution_multiply_fusion.8
  366.1 1.3 convolution_multiply_fusion.8
  383.9 3.7 fusion.41
  387.7 4.9 %fusion.38 = f32[512,512]{1,0:T(8,128)} fusion(f32[512,512]{1,0:T(8,128)} %fusion.41, bf16[4,512,512]{2,1,0:T(8,128)(2,1)} %all-gather.7.cloned.1.call-done, bf16[4,512,512]{2,1,0:T(8,128)(2,1)} %bitcast.284), kind=kOutput, calls=%fused_computation.73 | convolution fusion | flops 1074003968 | bytes 6291456 | tf_op jit(solution)/shard_map/ntc,ncd->td/dot_general | solution.py:232
  392.6 8.2 %all-gather.5.cloned.1.call-done = bf16[4,512,256]{2,1,0:T(8,128)(2,1)} async-done(((bf16[1,512,256]{2,1,0:T(8,128)(2,1)}), bf16[4,512,256]{2,1,0:T(8,128)(2,1)}) %all-gather.5.cloned.1.call-update) | async-done | bytes 1048592 | tf_op jit(solution)/shard_map/all_gather | solution.py:228
  400.8 3.0 fusion.43
  (290 shorter events, 125.6 us)
Async XLA Ops:
  6.5 189.8 %copy-start = (bf16[2048,512]{1,0:T(8,128)(2,1)S(1)}, bf16[2048,512]{1,0:T(8,128)(2,1)}, u32[]{:S(2)}) copy-start(bf16[2048,512]{1,0:T(8,128)(2,1)} %param.38) | copy-start | bytes 6291460
  9.6 13.7 %all-to-all-start = ((s32[8,1,4]{2,1,0:T(1,128)}), s32[8,1,4]{2,1,0:T(1,128)S(1)}, u32[]{:S(2)}, u32[]{:S(2)}) async-start(s32[8,1,4]{2,1,0:T(1,128)} %copy.148), calls=%async_computation | async-start | bytes 8192 | tf_op jit(solution)/shard_map/all_to_all | solution.py:192
  25.9 74.0 %all-to-all-start.1 = ((bf16[8,4,24,2048]{3,2,1,0:T(8,128)(2,1)}), bf16[8,4,24,2048]{3,2,1,0:T(8,128)(2,1)}, u32[]{:S(2)}, u32[]{:S(2)}) async-start(bf16[8,4,24,2048]{3,2,1,0:T(8,128)(2,1)} %bitcast.271), calls=%async_computation.1 | async-start | bytes 6291456 | tf_op jit(solution)/shard_map/all_to_all | solution.py:198
  30.3 155.2 %all-gather.9.cloned.1.call-start = ((), (), s32[]{:S(2)}) async-start(), calls=%async_computation.4 | async-start | bytes 15728640 | tf_op jit(solution)/shard_map/all_gather | solution.py:200
  104.2 283.5 %all-gather.7.cloned.1.call-start = ((), (), s32[]{:S(2)}) async-start(), calls=%async_computation.3 | async-start | bytes 2621440 | tf_op jit(solution)/shard_map/all_gather | solution.py:234
  108.3 4.2 %copy-start.7 = (f32[512]{0:T(512)S(1)}, f32[512]{0:T(512)}, u32[]{:S(2)}) copy-start(f32[512]{0:T(512)} %param.36) | copy-start | bytes 6148
  117.2 1.9 copy-start.11
  119.0 4.2 %copy-start.6 = (f32[512,4]{0,1:T(4,128)S(1)}, f32[512,4]{0,1:T(4,128)}, u32[]{:S(2)}) copy-start(f32[512,4]{0,1:T(4,128)} %param.30) | copy-start | bytes 24580
  121.8 1.7 copy-start.12
  136.3 3.0 copy-start.3
  136.3 3.0 copy-start.4
  232.9 5.6 %copy-start.5 = (bf16[8,64,2,256]{1,0,3,2:T(8,128)(2,1)S(1)}, bf16[8,64,2,256]{1,0,3,2:T(8,128)(2,1)}, u32[]{:S(2)}) copy-start(bf16[8,64,2,256]{1,0,3,2:T(8,128)(2,1)} %reshape.416) | copy-start | bytes 1572868
  247.0 2.9 copy-start.2
  249.8 151.0 %all-gather.5.cloned.1.call-start = ((), (), s32[]{:S(2)}) async-start(), calls=%async_computation.2 | async-start | bytes 1310720 | tf_op jit(solution)/shard_map/all_gather | solution.py:228
  382.1 0.8 copy-start.8
  382.6 1.3 copy-start.10
  382.6 1.3 copy-start.13
  387.6 13.1 %copy-start.9 = (bf16[1024,512]{1,0:T(8,128)(2,1)S(1)}, bf16[1024,512]{1,0:T(8,128)(2,1)}, u32[]{:S(2)}) copy-start(bf16[1024,512]{1,0:T(8,128)(2,1)} %param.34) | copy-start | bytes 3145732
  387.7 16.2 %copy-start.1 = (bf16[2048,512]{1,0:T(8,128)(2,1)S(1)}, bf16[2048,512]{1,0:T(8,128)(2,1)}, u32[]{:S(2)}) copy-start(bf16[2048,512]{1,0:T(8,128)(2,1)} %param.38) | copy-start | bytes 6291460
Sparse Core Ops, SparseCore 0:
  104.3 81.1 all-gather.8
  249.9 22.5 all-gather.6
  384.0 16.6 all-gather.4
where the time goes:
time: 413 us; the launch traced here: 410 us
  matrix products  187 us (45%)
  waiting for transfers between devices  127 us (31%)
  local copies, waits for them, and re-layouts  57 us (14%)
  between operations  13.5 us (3%)
  other arithmetic  12.5 us (3%)
  starting transfers between devices  11.8 us (3%)
    all_to_all x1, waiting for transfers between devices, local(): lax.all_to_all(outgoing, 'st', split_axis=0, concat_axis=0, tiled=True)  69.2 us
    all_gather x1, waiting for transfers between devices, local(): piece = lax.all_gather(picked, 'tp', axis=1, tiled=True)  44.1 us
    dot_general x32, matrix products, pair_dots(): return jnp.einsum('hsc,htc->hst', left, right, precision=PRECISE)  42.7 us
    dot_general x72, matrix products, apply_mat(): return jnp.einsum('hst,htc->hsc', matrix, vectors, precision=PRECISE)  34.4 us
    dot_general x1, matrix products, local(): jnp.dot(flat_rows, passage_value, preferred_element_type=FLOAT32)  11.2 us
    dot_general x8, matrix products, block_step(): jnp.einsum('hsi,hsj->hij', solved, rate_key * fade_out, precision=PRECISE)  10.4 us
    dot_general x40, matrix products, block_step(): jnp.einsum('hst,htu->hsu', power_mat, power_mat, precision=PRECISE)  10.2 us
    dot_general x8, matrix products, block_step(): jnp.einsum('hsj,hij->hsi', query_scaled, state, precision=PRECISE)  10.1 us
  transfers between devices with their start and end apart: 5, of which 4 were waited for; matrix products, arithmetic and copies ran while one was open for 44% of the time, Pallas kernels for 0%

commit v1 on v0

v1 whole, which is shorter than its diff:
```python
import functools

import jax
import jax.numpy as jnp
from jax import lax
from jax.experimental import pallas as pl
from jax.experimental.pallas import tpu as pltpu
from jax.sharding import PartitionSpec as P


XHEAD = 256
QBLOCK = 64
MBLOCK = 64


FLOAT32 = jnp.float32
BFLOAT = jnp.bfloat16


def head_norm(values, head_size):
    shaped = values.reshape(values.shape[:-1] + (values.shape[-1] // head_size, head_size))
    scaled = shaped * lax.rsqrt(jnp.mean(shaped * shaped, axis=-1, keepdims=True) + 1e-06)
    return scaled.reshape(values.shape)


def split(values):
    high = values.astype(BFLOAT)
    return high, (values - high.astype(FLOAT32)).astype(BFLOAT)


def raw_dot(left, right, dims):
    return lax.dot_general(left, right, (dims, ((), ())), preferred_element_type=FLOAT32)


def fine_dot(left, right, dims=((1,), (0,))):
    left_high, left_low = left if isinstance(left, tuple) else split(left)
    right_high, right_low = right if isinstance(right, tuple) else split(right)
    return raw_dot(left_high, right_high, dims) + (
        raw_dot(left_high, right_low, dims) + raw_dot(left_low, right_high, dims)
    )


def exact_dot(values, ones):
    high, low = split(values)
    return raw_dot(high, ones, ((1,), (0,))) + raw_dot(low, ones, ((1,), (0,)))


def mixer_kernel(
    heads, blocks, query_ref, key_ref, value_ref, fade_ref, gate_ref, gain_ref, out_ref, state_ref
):
    width = query_ref.shape[1]
    size = width // heads
    rows = heads * MBLOCK

    @pl.when(pl.program_id(0) == 0)
    def _():
        state_ref[...] = jnp.zeros_like(state_ref)

    def iota(shape, dim):
        return lax.broadcasted_iota(jnp.int32, shape, dim)

    row_head = (iota((rows, width), 0) // MBLOCK) == (iota((rows, width), 1) // size)
    state_head = (iota((width, width), 0) // size) == (iota((width, width), 1) // size)
    ones_head = jnp.where(state_head, 1.0, 0.0).astype(BFLOAT)
    row_pos = iota((rows, rows), 0) % MBLOCK
    col_pos = iota((rows, rows), 1) % MBLOCK
    strict = col_pos < row_pos
    upto = col_pos <= row_pos
    lower = jnp.where(
        iota((MBLOCK, MBLOCK), 1) <= iota((MBLOCK, MBLOCK), 0), 1.0, 0.0
    ).astype(BFLOAT)

    def expand(values):
        return jnp.where(row_head, jnp.concatenate([values] * heads, axis=0), 0.0)

    def compact(values):
        return jnp.concatenate(
            [values[:, head * size : (head + 1) * size] for head in range(heads)], axis=0
        )

    def natural(values):
        return jnp.concatenate(
            [values[head * MBLOCK : (head + 1) * MBLOCK] for head in range(heads)], axis=1
        )

    def each(fn, *lists):
        return [fn(*items) for items in zip(*lists)]

    def load(ref):
        return [ref[pl.ds(b * MBLOCK, MBLOCK), :].astype(FLOAT32) for b in range(blocks)]

    def running_sum(fade):
        high, low = split(fade)
        rest = (fade - high.astype(FLOAT32) - low.astype(FLOAT32)).astype(BFLOAT)
        dims = ((1,), (0,))
        return raw_dot(lower, high, dims) + (raw_dot(lower, low, dims) + raw_dot(lower, rest, dims))

    query, key, value = load(query_ref), load(key_ref), load(value_ref)
    fade, gate = load(fade_ref), load(gate_ref)
    cumul = each(running_sum, fade)
    unit = each(lambda k: k * lax.rsqrt(exact_dot(k * k, ones_head) + 1e-06), key)
    rate = each(lambda u, g: u * g, unit, gate)
    minus_scaled = each(lambda u, c, f: -u * jnp.exp(c - f), unit, cumul, fade)
    query_scaled = each(lambda q, c: q * jnp.exp(c), query, cumul)
    inverse = each(lambda c: jnp.exp(-c), cumul)
    fade_out = each(lambda c: jnp.exp(c[MBLOCK - 1 :, :] - c), cumul)
    block_fade = each(lambda c: jnp.exp(c[MBLOCK - 1 :, :]), cumul)
    left = each(
        lambda m, q: split(jnp.concatenate([expand(m), expand(q)], axis=0)),
        minus_scaled,
        query_scaled,
    )
    right = each(
        lambda k, r, i: split(jnp.concatenate([expand(k * i), expand(r * i)], axis=0)),
        key,
        rate,
        inverse,
    )
    pairs = each(lambda a, b: fine_dot(a, b, ((1,), (1,))), left, right)
    key_mats = each(
        lambda p: jnp.concatenate(
            [jnp.where(strict, p[:rows, :rows], 0.0), jnp.where(upto, p[rows:, :rows], 0.0)], axis=0
        ),
        pairs,
    )
    rate_pull = each(lambda p: split(jnp.where(strict, p[:rows, rows:], 0.0)), pairs)
    rate_read = each(lambda p: split(jnp.where(upto, p[rows:, rows:], 0.0)), pairs)
    value_rows = each(lambda v: compact(v).astype(BFLOAT), value)

    def key_values(mats, vals):
        high, low = split(mats)
        return raw_dot(high, vals, ((1,), (0,))) + raw_dot(low, vals, ((1,), (0,)))

    from_values = each(key_values, key_mats, value_rows)
    solved = each(
        lambda m, kv: jnp.concatenate([compact(m), kv[:rows]], axis=1), minus_scaled, from_values
    )
    power = rate_pull
    levels = (MBLOCK - 1).bit_length()
    for level in range(levels):
        solved = each(lambda s, p: s + fine_dot(p, s), solved, power)
        if level < levels - 1:
            power = each(lambda p: split(fine_dot(p, p)), power)
    solved_halves = each(split, solved)
    reads = each(
        lambda q, kv, r, s: jnp.concatenate([compact(q), kv[rows:]], axis=1) + fine_dot(r, s),
        query_scaled,
        from_values,
        rate_read,
        solved_halves,
    )
    moved = each(
        lambda s, r, f: fine_dot(s, expand(r * f), ((0,), (0,))), solved_halves, rate, fade_out
    )

    def key_update(vals, k, f):
        high, low = split(expand(k * f))
        dims = ((0,), (0,))
        return raw_dot(vals, high, dims) + raw_dot(vals, low, dims)

    added = each(key_update, value_rows, key, fade_out)
    carry = each(
        lambda m: split(jnp.where(state_head, jnp.concatenate([m[:size]] * heads, axis=0), 0.0)),
        moved,
    )
    added = each(lambda a, m: a + m[size:], added, moved)
    read_state = each(lambda r: split(natural(r[:, :size])), reads)
    read_fixed = each(lambda r: natural(r[:, size:]), reads)
    state = state_ref[...]
    head_out = []
    for block in range(blocks):
        spread_state = jnp.where(state_head, jnp.concatenate([state] * heads, axis=0), 0.0)
        head_out.append(
            read_fixed[block] + fine_dot(read_state[block], spread_state, ((1,), (1,)))
        )
        state = state * block_fade[block] + fine_dot(state, carry[block]) + added[block]
    state_ref[...] = state
    for block in range(blocks):
        mean = exact_dot(head_out[block], ones_head) * (1.0 / size)
        centred = head_out[block] - mean
        variance = exact_dot(centred * centred, ones_head) * (1.0 / size)
        normed = centred * lax.rsqrt(variance + 0.00064) * gain_ref[...]
        out_ref[pl.ds(block * MBLOCK, MBLOCK), :] = normed.astype(BFLOAT)


def recurrence(heads, query_vec, key_vec, value_vec, log_fade, rate_gate, norm_gain):
    rows, width = query_vec.shape
    blocks = 2 if rows % (2 * MBLOCK) == 0 else 1
    step = blocks * MBLOCK
    piece = pl.BlockSpec((step, width), lambda i: (i, 0))
    return pl.pallas_call(
        functools.partial(mixer_kernel, heads, blocks),
        grid=(rows // step,),
        in_specs=[piece] * 5 + [pl.BlockSpec((1, width), lambda i: (0, 0))],
        out_specs=piece,
        out_shape=jax.ShapeDtypeStruct((rows, width), BFLOAT),
        scratch_shapes=[pltpu.VMEM((width // heads, width), FLOAT32)],
        compiler_params=pltpu.CompilerParams(
            dimension_semantics=("arbitrary",), vmem_limit_bytes=48 * 1024 * 1024
        ),
        cost_estimate=pl.CostEstimate(
            flops=rows * width * 40000, bytes_accessed=rows * width * 16, transcendentals=0
        ),
    )(query_vec, key_vec, value_vec, log_fade, rate_gate, norm_gain.reshape(1, width))


def partial_kernel(heads, per_step, ids_ref, query_ref, key_ref, value_ref, out_ref, sum_ref):
    base = pl.program_id(0) * per_step
    length = key_ref.shape[1]
    ones = jnp.ones((8, length), BFLOAT)
    for slot in range(per_step):
        passage = ids_ref[base + slot]
        for head in range(heads):
            span = pl.ds(head * XHEAD, XHEAD)
            scores = raw_dot(
                query_ref[slot, :, span], key_ref[passage, :, span], ((1,), (1,))
            ) * XHEAD ** (-0.5)
            expon = jnp.exp(scores).astype(BFLOAT)
            out_ref[slot, :, span] = raw_dot(
                expon, value_ref[passage, :, span], ((1,), (0,))
            ).astype(BFLOAT)
            sums = raw_dot(ones, expon, ((1,), (1,)))
            sum_ref[slot, pl.ds(head, 1), :] = sums[:1]


def partial_attention(ids, queries, keys, values):
    slots, tokens, width = queries.shape
    heads = width // XHEAD
    per_step = 4 if slots % 4 == 0 else 2
    whole = pl.BlockSpec(keys.shape, lambda i, ids: (0, 0, 0))
    return pl.pallas_call(
        functools.partial(partial_kernel, heads, per_step),
        grid_spec=pltpu.PrefetchScalarGridSpec(
            num_scalar_prefetch=1,
            grid=(slots // per_step,),
            in_specs=[
                pl.BlockSpec((per_step, tokens, width), lambda i, ids: (i, 0, 0)),
                whole,
                whole,
            ],
            out_specs=[
                pl.BlockSpec((per_step, tokens, width), lambda i, ids: (i, 0, 0)),
                pl.BlockSpec((per_step, heads, tokens), lambda i, ids: (i, 0, 0)),
            ],
        ),
        out_shape=[
            jax.ShapeDtypeStruct((slots, tokens, width), BFLOAT),
            jax.ShapeDtypeStruct((slots, heads, tokens), FLOAT32),
        ],
        compiler_params=pltpu.CompilerParams(
            dimension_semantics=("arbitrary",), vmem_limit_bytes=32 * 1024 * 1024
        ),
        cost_estimate=pl.CostEstimate(
            flops=slots * tokens * width * keys.shape[1] * 4,
            bytes_accessed=slots * tokens * width * 4,
            transcendentals=0,
        ),
    )(ids, queries, keys, values)


def combine_kernel(heads, where_ref, *refs):
    *part_refs, scale_ref, out_ref = refs
    for head in range(heads):
        span = pl.ds(head * XHEAD, XHEAD)
        total = part_refs[0][0, :, span].astype(FLOAT32)
        for part in part_refs[1:]:
            total = total + part[0, :, span].astype(FLOAT32)
        out_ref[:, span] = (total * scale_ref[0, :, head : head + 1]).astype(BFLOAT)


def combine(where, parts, scale):
    blocks, per_block = where.shape
    _, tokens, width = parts.shape
    heads = width // XHEAD

    def part_spec(place):
        return pl.BlockSpec(
            (1, tokens, width), lambda i, where: (where[i * per_block + place], 0, 0)
        )

    return pl.pallas_call(
        functools.partial(combine_kernel, heads),
        grid_spec=pltpu.PrefetchScalarGridSpec(
            num_scalar_prefetch=1,
            grid=(blocks,),
            in_specs=[part_spec(place) for place in range(per_block)]
            + [pl.BlockSpec((1, tokens, heads), lambda i, where: (i, 0, 0))],
            out_specs=pl.BlockSpec((tokens, width), lambda i, where: (i, 0)),
        ),
        out_shape=jax.ShapeDtypeStruct((blocks * tokens, width), BFLOAT),
        compiler_params=pltpu.CompilerParams(dimension_semantics=("arbitrary",)),
    )(where.reshape(-1), *([parts] * per_block), scale)


def mixer(
    tokens,
    mix_query,
    mix_key,
    mix_value,
    decay_lower_map,
    decay_upper_map,
    decay_base,
    decay_shift,
    rate_lower_map,
    rate_upper_map,
    norm_gain,
):
    head_count = decay_shift.shape[1]
    head_size = mix_query.shape[1] // head_count

    def project(weight):
        return jnp.dot(tokens, weight, preferred_element_type=FLOAT32).astype(BFLOAT)

    query_vec = project(mix_query)
    key_vec = project(mix_key)
    value_vec = project(mix_value)
    decay_low = jnp.tanh(
        jnp.dot(tokens, decay_lower_map, preferred_element_type=FLOAT32)
    ).astype(BFLOAT)
    decay_pre = (
        decay_base
        + jnp.dot(decay_low, decay_upper_map, preferred_element_type=FLOAT32)
        + jnp.repeat(decay_shift, head_size, axis=1)
    )
    log_fade = -jnp.exp(-jax.nn.softplus(-decay_pre) - 0.5)
    rate_low = jnp.dot(tokens, rate_lower_map, preferred_element_type=FLOAT32).astype(BFLOAT)
    rate_gate = jax.nn.sigmoid(jnp.dot(rate_low, rate_upper_map, preferred_element_type=FLOAT32))
    return recurrence(
        head_count, query_vec, key_vec, value_vec, log_fade, rate_gate, norm_gain
    )


def layer(
    tokens,
    mix_query,
    mix_key,
    mix_value,
    decay_lower_map,
    decay_upper_map,
    decay_base,
    decay_shift,
    rate_lower_map,
    rate_upper_map,
    norm_gain,
    mix_out,
    cross_query,
    score_gain,
    passage_key,
    passage_value,
    cross_out,
    gate_down,
    gate_up,
    store,
    passage_ids,
):
    model_width = tokens.shape[1]
    owner_count = lax.axis_size("st")
    pass_dev = store.shape[0]
    passage_len = store.shape[1]
    cross_width = cross_query.shape[1]
    head_count = cross_width // XHEAD
    block_count, per_block = passage_ids.shape
    flat_ids = passage_ids.reshape(-1)
    slot_count = flat_ids.shape[0]
    capacity = max(2, -(-slot_count // owner_count))
    owner_of = flat_ids // pass_dev
    local_idx = flat_ids % pass_dev
    slot_order = jnp.arange(slot_count)
    earlier_same = (owner_of[:, None] == owner_of[None, :]) & (
        slot_order[None, :] < slot_order[:, None]
    )
    slot_rank = jnp.sum(earlier_same.astype(jnp.int32), axis=1)
    to_owner = owner_of[:, None] == jnp.arange(owner_count)[None, :]
    to_slot = slot_rank[:, None] == jnp.arange(capacity)[None, :]
    chosen = to_owner[:, :, None] & to_slot[:, None, :]
    wanted = jnp.sum(jnp.where(chosen, local_idx[:, None, None], 0), axis=0)
    asking = jnp.sum(jnp.where(chosen, (slot_order // per_block)[:, None, None], 0), axis=0)
    where_from = owner_of * capacity + slot_rank

    served = lax.all_to_all(wanted, "st", split_axis=0, concat_axis=0, tiled=True).reshape(-1)
    queries = (
        head_norm(jnp.dot(tokens, cross_query, preferred_element_type=FLOAT32), XHEAD)
        * score_gain
    )
    queries = queries.astype(BFLOAT).reshape(block_count, QBLOCK, cross_width)
    outgoing = queries[asking.reshape(-1)].reshape(
        owner_count, capacity, QBLOCK, cross_width
    )
    incoming = lax.all_to_all(outgoing, "st", split_axis=0, concat_axis=0, tiled=True)
    flat_rows = store.reshape(-1, model_width)
    keyed = head_norm(
        jnp.dot(flat_rows, passage_key, preferred_element_type=FLOAT32), XHEAD
    ).astype(BFLOAT)
    valued = jnp.dot(flat_rows, passage_value, preferred_element_type=FLOAT32).astype(BFLOAT)
    keyed = keyed.reshape(pass_dev, passage_len, cross_width)
    valued = valued.reshape(pass_dev, passage_len, cross_width)
    parts, sums = partial_attention(
        served,
        incoming.reshape(owner_count * capacity, QBLOCK, cross_width),
        keyed,
        valued,
    )
    sums = lax.all_to_all(
        sums.reshape(owner_count, capacity, head_count, QBLOCK),
        "st",
        split_axis=0,
        concat_axis=0,
        tiled=True,
    )
    parts = lax.all_to_all(
        parts.reshape(owner_count, capacity, QBLOCK, cross_width),
        "st",
        split_axis=0,
        concat_axis=0,
        tiled=True,
    )
    mixer_heads = mixer(
        tokens,
        mix_query,
        mix_key,
        mix_value,
        decay_lower_map,
        decay_upper_map,
        decay_base,
        decay_shift,
        rate_lower_map,
        rate_upper_map,
        norm_gain,
    )
    sums = sums.reshape(owner_count * capacity, head_count, QBLOCK)[where_from]
    sums = jnp.sum(sums.reshape(block_count, per_block, head_count, QBLOCK), axis=1)
    scale = (1.0 / sums).transpose(0, 2, 1)
    attended = combine(
        where_from.reshape(block_count, per_block),
        parts.reshape(owner_count * capacity, QBLOCK, cross_width),
        scale,
    )
    shard_total = lax.axis_size("tp")
    out_cols = mix_out.shape[1]
    mix_rows = mix_out.reshape(shard_total, -1, out_cols)
    cross_rows = cross_out.reshape(shard_total, -1, out_cols)
    mixer_part = jnp.einsum(
        "ntc,ncd->td",
        lax.all_gather(mixer_heads[None], "tp", axis=0, tiled=True),
        mix_rows,
        preferred_element_type=FLOAT32,
    )
    gate_low = jnp.dot(tokens, gate_down, preferred_element_type=FLOAT32).astype(BFLOAT)
    gate_open = jax.nn.sigmoid(jnp.dot(gate_low, gate_up, preferred_element_type=FLOAT32))
    cross_part = jnp.einsum(
        "ntc,ncd->td",
        lax.all_gather(attended[None], "tp", axis=0, tiled=True),
        cross_rows,
        preferred_element_type=FLOAT32,
    )
    return (mixer_part + gate_open * cross_part).astype(BFLOAT)


def solution(mesh):
    placed = (
        P("st", None),
        P(None, "tp"),
        P(None, "tp"),
        P(None, "tp"),
        P(),
        P(None, "tp"),
        P("tp"),
        P("st", "tp"),
        P(),
        P(None, "tp"),
        P("tp"),
        P(None, "tp"),
        P(None, "tp"),
        P("tp"),
        P(None, "tp"),
        P(None, "tp"),
        P(None, "tp"),
        P(),
        P(None, "tp"),
        P("st", None, None),
        P("st", None),
    )
    return jax.shard_map(
        layer, mesh=mesh, in_specs=placed, out_specs=P("st", "tp"), check_vma=False
    )
```

time: 413 us -> 223 us (0.54)
  matrix products: 187 us -> 35.3 us
  waiting for transfers between devices: 127 us -> 75.2 us
  Pallas kernels: 0 us -> 39.7 us
  local copies, waits for them, and re-layouts: 57 us -> 25.1 us
  blocking collectives: 0 us -> 10 us
  other arithmetic: 12.5 us -> 5.05 us
  starting transfers between devices: 11.8 us -> 17.9 us
    dot_general x187 -> x9, matrix products: 181 us -> 30 us  [the longest x1 6.65 us: layer(): jnp.dot(flat_rows, passage_value, preferred_element_type=FLOAT32)]
    all_gather x3 -> x2, waiting for transfers between devices: 52.3 us -> 7.73 us  [the longest x1 7.73 us: layer(): lax.all_gather(mixer_heads[None], 'tp', axis=0, tiled=True)]
    pallas_call x0 -> x3, Pallas kernels: none -> 39.7 us  [the longest x1 23.8 us: recurrence(): pl.pallas_call(functools.partial(mixer_kernel, heads, blocks), grid=(rows...]
    reshape x7 -> x2, local copies, waits for them, and re-layouts: 17.3 us -> 0.16 us  [the longest x1 0.08 us: layer(): asking.reshape(-1)]
    all_to_all x0 -> x1, blocking collectives: none -> 10 us  [layer(): lax.all_to_all(sums.reshape(owner_count, capacity, head_count, QBLOCK), '...]
    concatenate x1 -> x0, local copies, waits for them, and re-layouts: 8.62 us -> none  [local(): joined = jnp.concatenate([keyed, valued], axis=-1)]
    all_to_all x2 -> x3, waiting for transfers between devices: 74.3 us -> 67.5 us  [the longest x1 43.5 us: layer(): lax.all_to_all(parts.reshape(owner_count, capacity, QBLOCK, cross_width),...]
    transpose x5 -> x0, local copies, waits for them, and re-layouts: 6.63 us -> none  [the longest x4 6.25 us: to_blocks(): return shaped.transpose(0, 2, 1, 3)]
  transfers between devices with their start and end apart: 5 -> 5, of which waited for: 4 -> 3; matrix products, arithmetic and copies ran while one was open for 44% -> 24% of each run, Pallas kernels for 0% -> 11%
where the time goes in v1:
time: 223 us; the launch traced here: 222 us
  waiting for transfers between devices  75.2 us (34%)
  Pallas kernels  39.7 us (18%)
  matrix products  35.3 us (16%)
  local copies, waits for them, and re-layouts  25.1 us (11%)
  starting transfers between devices  17.9 us (8%)
  between operations  13.7 us (6%)
  blocking collectives  10 us (4%)
  other arithmetic  5.05 us (2%)
    all_to_all x1, waiting for transfers between devices, layer(): lax.all_to_all(parts.reshape(owner_count, capacity, QBLOCK, cross_width),...  43.5 us
    all_to_all x1, waiting for transfers between devices, layer(): lax.all_to_all(outgoing, 'st', split_axis=0, concat_axis=0, tiled=True)  23.9 us
    pallas_call x1, Pallas kernels, recurrence(): pl.pallas_call(functools.partial(mixer_kernel, heads, blocks), grid=(rows...  23.8 us
    all_to_all x1, blocking collectives, layer(): lax.all_to_all(sums.reshape(owner_count, capacity, head_count, QBLOCK), '...  10 us
    pallas_call x1, Pallas kernels, partial_attention(): pl.pallas_call(functools.partial(partial_kernel, heads, per_step), grid_s...  9.51 us
    all_gather x1, waiting for transfers between devices, layer(): lax.all_gather(mixer_heads[None], 'tp', axis=0, tiled=True)  7.73 us
    all_to_all x1, starting transfers between devices, layer(): lax.all_to_all(wanted, 'st', split_axis=0, concat_axis=0, tiled=True)  7.28 us
    dot_general x1, matrix products, layer(): jnp.dot(flat_rows, passage_value, preferred_element_type=FLOAT32)  6.65 us
  transfers between devices with their start and end apart: 5, of which 3 were waited for; matrix products, arithmetic and copies ran while one was open for 24% of the time, Pallas kernels for 11%

profile of v1, /device:TPU:0, one launch (start us, length us, event | category | flops | bytes accessed | tf_op | source)
XLA Modules:
  0.0 221.9 jit_solution(10836570330160467703)
XLA Ops:
  6.5 0.8 broadcast_remainder_fusion
  7.4 0.7 compare_and_fusion
  8.8 0.2 fusion.17
  9.0 0.7 copy.80
  9.7 7.3 %all-to-all-start = ((s32[8,1,4]{2,1,0:T(1,128)}), s32[8,1,4]{2,1,0:T(1,128)S(1)}, u32[]{:S(2)}, u32[]{:S(2)}) async-start(s32[8,1,4]{2,1,0:T(1,128)} %copy.80), calls=%async_computation | async-start | bytes 8192 | tf_op jit(solution)/shard_map/all_to_all | solution.py:380
  17.2 4.1 %fusion.23 = (f32[512,512]{1,0:T(8,128)}, f32[512,512]{1,0:T(8,128)}) fusion(bf16[512,2048]{1,0:T(8,128)(2,1)S(1)} %copy-done, bf16[2048,512]{1,0:T(8,128)(2,1)} %param.33), kind=kOutput, calls=%fused_computation.67 | convolution fusion | flops 1074003968 | bytes 6291456 | tf_op jit(solution)/shard_map/dot_general | solution.py:382
  21.3 1.9 mul.59
  23.2 0.6 reduce_sum.58
  23.9 0.6 mul.60
  24.6 0.5 copy-done.5
  25.0 0.3 multiply_convert_fusion.1
  25.3 2.0 gather_fusion
  27.3 6.0 %all-to-all-start.1 = ((bf16[8,4,64,512]{3,2,1,0:T(8,128)(2,1)}), bf16[8,4,64,512]{3,2,1,0:T(8,128)(2,1)}, u32[]{:S(2)}, u32[]{:S(2)}) async-start(bf16[8,4,64,512]{3,2,1,0:T(8,128)(2,1)} %bitcast.73), calls=%async_computation.1 | async-start | bytes 4194304 | tf_op jit(solution)/shard_map/all_to_all | solution.py:389
  33.3 4.0 %copy.90 = bf16[512,2048]{1,0:T(8,128)(2,1)} copy(bf16[512,2048]{0,1:T(8,128)(2,1)} %bitcast.76) | data formatting | bytes 4194304 | tf_op jit(solution)/shard_map/dot_general | solution.py:392
  37.3 6.0 %multiply_reduce_fusion = (f32[1152,2]{0,1:T(2,128)S(1)}, f32[1152,2,256]{0,2,1:T(8,128)S(1)}) fusion(bf16[1152,2048,1]{1,0,2:T(8,128)(2,1)} %bitcast.82, bf16[2,256,2048]{2,1,0:T(8,128)(2,1)} %bitcast.77), kind=kOutput, calls=%fused_computation.4 | convolution fusion | flops 2417096448 | bytes 9184256 | tf_op jit(solution)/shard_map/dot_general | solution.py:392
  43.4 2.7 %copy.85 = bf16[1152,2,256]{2,1,0:T(2,128)(2,1)} copy(bf16[1152,2,256]{0,2,1:T(8,128)(2,1)S(1)} %multiply_convert_fusion) | data formatting | bytes 2359296 | tf_op jit(solution)/shard_map/convert_element_type | solution.py:393
  46.1 3.1 %convert_element_type.46.key_ref = bf16[12,96,512]{2,1,0:T(8,128)(2,1)S(1)} reshape(bf16[1152,2,256]{2,1,0:T(2,128)(2,1)} %copy.85) | data formatting | bytes 2359296 | tf_op jit(solution)/shard_map/convert_element_type | solution.py:393
  49.3 6.7 %convolution_convert_fusion = bf16[1152,512]{1,0:T(8,128)(2,1)} fusion(bf16[1152,2048]{1,0:T(8,128)(2,1)} %bitcast.83, bf16[2048,512]{1,0:T(8,128)(2,1)} %param.36), kind=kOutput, calls=%fused_computation.2 | convolution fusion | flops 2416508928 | bytes 7995392 | tf_op jit(solution)/shard_map/dot_general | solution.py:394
  55.9 0.5 broadcast.246
  56.4 0.7 reduce.3
  57.2 23.9 %all-to-all-done.1 = bf16[8,4,64,512]{3,2,1,0:T(8,128)(2,1)} async-done(((bf16[8,4,64,512]{3,2,1,0:T(8,128)(2,1)}), bf16[8,4,64,512]{3,2,1,0:T(8,128)(2,1)}, u32[]{:S(2)}, u32[]{:S(2)}) %all-to-all-start.1) | async-done | bytes 2097184 | tf_op jit(solution)/shard_map/all_to_all | solution.py:389
  81.1 1.3 copy-done.2
  82.4 9.5 %shard_map.200 = (bf16[32,64,512]{2,1,0:T(8,128)(2,1)S(1)}, f32[32,2,64]{2,1,0:T(2,128)S(1)}) custom-call(s32[32]{0:T(128)S(1)} %reshape.275.ids_ref, bf16[32,64,512]{2,1,0:T(8,128)(2,1)} %bitcast.9.query_ref, bf16[12,96,512]{2,1,0:T(8,128)(2,1)S(1)} %convert_element_type.46.key_ref, bf16[12,96,512]{2,1,0:T(8,128)(2,1)S(1)} %bitcast.69), custom_call_target="tpu_custom_call" | custom-call | flops 402653184 | bytes 4194304 | tf_op jit(solution)/shard_map/pallas_call | solution.py:231
  91.9 1.3 copy-done.1
  93.3 10.0 %all_to_all.24 = f32[8,1,512]{2,1,0:T(1,128)S(1)} all-to-all(f32[8,1,512]{2,1,0:T(1,128)S(1)} %reshape.318), channel_id=1, replica_groups=mesh['st'=8,'tp'=4] {'st'}, dimensions={0} | all-to-all | bytes 32768 | tf_op jit(solution)/shard_map/all_to_all | solution.py:403
  103.3 4.4 %all-to-all-start.2 = ((bf16[8,4,64,512]{3,2,1,0:T(8,128)(2,1)}), bf16[8,4,64,512]{3,2,1,0:T(8,128)(2,1)}, u32[]{:S(2)}, u32[]{:S(2)}) async-start(bf16[8,4,64,512]{3,2,1,0:T(8,128)(2,1)} %bitcast.68), calls=%async_computation.2 | async-start | bytes 4194304 | tf_op jit(solution)/shard_map/all_to_all | solution.py:410
  108.0 0.6 multiply_add_fusion.where_ref
  108.6 0.5 broadcast.247
  109.1 0.7 reduce.4
  109.9 0.6 gather_fusion.1
  110.6 0.9 copy.89
  111.4 43.5 %all-to-all-done.2 = bf16[8,4,64,512]{3,2,1,0:T(8,128)(2,1)} async-done(((bf16[8,4,64,512]{3,2,1,0:T(8,128)(2,1)}), bf16[8,4,64,512]{3,2,1,0:T(8,128)(2,1)}, u32[]{:S(2)}, u32[]{:S(2)}) %all-to-all-start.2) | async-done | bytes 2097184 | tf_op jit(solution)/shard_map/all_to_all | solution.py:410
  155.0 6.4 %shard_map.201 = bf16[512,512]{1,0:T(8,128)(2,1)} custom-call(s32[32]{0:T(128)} %multiply_add_fusion.where_ref, bf16[32,64,512]{2,1,0:T(8,128)(2,1)} %bitcast.16.refs_0_.refs_1_.refs_2_.refs_3_, bf16[32,64,512]{2,1,0:T(8,128)(2,1)} %bitcast.16.refs_0_.refs_1_.refs_2_.refs_3_, bf16[32,64,512]{2,1,0:T(8,128)(2,1)} %bitcast.16.refs_0_.refs_1_.refs_2_.refs_3_, ...), custom_call_target="tpu_custom_call" | custom-call | tf_op jit(solution)/shard_map/pallas_call | solution.py:281
  161.3 0.2 all-gather.5.cloned.1.call-start
  161.6 1.0 copy.76
  162.6 2.9 %fusion.8.gate_ref = f32[512,256]{1,0:T(8,128)} fusion(bf16[64,256]{1,0:T(8,128)(2,1)S(1)} %copy-done.13, bf16[512,2048]{1,0:T(8,128)(2,1)S(1)} %copy-done, bf16[2048,64]{0,1:T(8,128)(2,1)} %param.29), kind=kOutput, calls=%fused_computation.18 | convolution fusion | flops 151420928 | bytes 2916352 | tf_op jit(solution)/shard_map/dot_general | solution.py:327
  165.5 0.7 convolution_convert_fusion.1.value_ref
  166.3 0.6 copy-done.9
  166.8 0.7 convolution_convert_fusion.2.key_ref
  167.5 0.6 copy-done.10
  168.1 0.7 convolution_convert_fusion.3.query_ref
  168.9 2.4 %fusion.15.fade_ref = f32[512,256]{1,0:T(8,128)S(1)} fusion(f32[512,256]{1,0:T(8,128)} %copy.76, bf16[64,256]{1,0:T(8,128)(2,1)S(1)} %copy-done.14, bf16[512,2048]{1,0:T(8,128)(2,1)S(1)} %copy-done, bf16[2048,64]{0,1:T(8,128)(2,1)} %param.25, f32[256]{0:T(256)S(1)} %copy-done.15), kind=kOutput, calls=%fused_computation.33 | convolution fusion | flops 152600576 | bytes 3441664 | tf_op jit(solution)/shard_map/dot_general | solution.py:322
  171.3 1.0 copy-done.4
  172.4 23.8 %shard_map.199 = bf16[512,256]{1,0:T(8,128)(2,1)} custom-call(bf16[512,256]{1,0:T(8,128)(2,1)S(1)} %convolution_convert_fusion.3.query_ref, bf16[512,256]{1,0:T(8,128)(2,1)S(1)} %convolution_convert_fusion.2.key_ref, bf16[512,256]{1,0:T(8,128)(2,1)S(1)} %convolution_convert_fusion.1.value_ref, f32[512,256]{1,0:T(8,128)S(1)} %fusion.15.fade_ref, ...), custom_call_target="tpu_custom_call" | custom-call | flops 5242880000 | bytes 2097152 | tf_op jit(solution)/shard_map/pallas_call | solution.py:191
  196.2 3.2 %fusion.3 = f32[512,512]{1,0:T(8,128)} fusion(bf16[128,512]{1,0:T(8,128)(2,1)S(1)} %copy-done.12, bf16[512,2048]{1,0:T(8,128)(2,1)S(1)} %copy-done, bf16[2048,128]{1,0:T(8,128)(2,1)} %param.38), kind=kOutput, calls=%fused_computation.11 | convolution fusion | flops 336396288 | bytes 3801088 | tf_op jit(solution)/shard_map/dot_general | solution.py:449
  199.4 4.9 %fusion = f32[512,512]{1,0:T(8,128)} fusion(f32[512,512]{1,0:T(8,128)} %fusion.3, bf16[4,512,512]{2,1,0:T(8,128)(2,1)} %bitcast.85, bf16[4,512,512]{2,1,0:T(8,128)(2,1)} %bitcast.84), kind=kOutput, calls=%fused_computation.7 | convolution fusion | flops 1074003968 | bytes 6291456 | tf_op jit(solution)/shard_map/ntc,ncd->td/dot_general | solution.py:450
  204.3 7.7 %all-gather.5.cloned.1.call-done = bf16[2048,256]{1,0:T(8,128)(2,1)} async-done(((bf16[512,256]{1,0:T(8,128)(2,1)}), bf16[2048,256]{1,0:T(8,128)(2,1)}) %all-gather.5.cloned.1.call-update) | async-done | bytes 1048592 | tf_op jit(solution)/shard_map/all_gather | solution.py:444
  212.0 3.0 %fusion.5 = bf16[512,512]{1,0:T(8,128)(2,1)} fusion(f32[512,512]{1,0:T(8,128)} %fusion, bf16[4,512,256]{2,1,0:T(8,128)(2,1)} %bitcast.87, bf16[4,256,512]{2,1,0:T(8,128)(2,1)S(1)} %bitcast.86), kind=kOutput, calls=%fused_computation.14 | convolution fusion | flops 537395200 | bytes 3670016 | tf_op jit(solution)/shard_map/ntc,ncd->td/dot_general | solution.py:442
  (60 shorter events, 2.0 us)
Async XLA Ops:
  6.5 10.6 %copy-start = (bf16[512,2048]{1,0:T(8,128)(2,1)S(1)}, bf16[512,2048]{1,0:T(8,128)(2,1)}, u32[]{:S(2)}) copy-start(bf16[512,2048]{1,0:T(8,128)(2,1)} %param.21) | copy-start | bytes 6291460
  9.7 17.6 %all-to-all-start = ((s32[8,1,4]{2,1,0:T(1,128)}), s32[8,1,4]{2,1,0:T(1,128)S(1)}, u32[]{:S(2)}, u32[]{:S(2)}) async-start(s32[8,1,4]{2,1,0:T(1,128)} %copy.80), calls=%async_computation | async-start | bytes 8192 | tf_op jit(solution)/shard_map/all_to_all | solution.py:380
  23.8 1.2 copy-start.5
  23.8 1.2 copy-start.7
  27.3 53.8 %all-to-all-start.1 = ((bf16[8,4,64,512]{3,2,1,0:T(8,128)(2,1)}), bf16[8,4,64,512]{3,2,1,0:T(8,128)(2,1)}, u32[]{:S(2)}, u32[]{:S(2)}) async-start(bf16[8,4,64,512]{3,2,1,0:T(8,128)(2,1)} %bitcast.73), calls=%async_computation.1 | async-start | bytes 4194304 | tf_op jit(solution)/shard_map/all_to_all | solution.py:389
  81.1 1.3 copy-start.2
  91.9 1.3 copy-start.1
  103.3 51.6 %all-to-all-start.2 = ((bf16[8,4,64,512]{3,2,1,0:T(8,128)(2,1)}), bf16[8,4,64,512]{3,2,1,0:T(8,128)(2,1)}, u32[]{:S(2)}, u32[]{:S(2)}) async-start(bf16[8,4,64,512]{3,2,1,0:T(8,128)(2,1)} %bitcast.68), calls=%async_computation.2 | async-start | bytes 4194304 | tf_op jit(solution)/shard_map/all_to_all | solution.py:410
  107.7 91.7 %all-gather.7.cloned.1.call-start = ((), (), s32[]{:S(2)}) async-start(), calls=%async_computation.5 | async-start | bytes 2621440 | tf_op jit(solution)/shard_map/all_gather | solution.py:452
  155.0 6.6 %copy-start.6 = (f32[512,4]{0,1:T(4,128)S(1)}, f32[512,4]{0,1:T(4,128)}, u32[]{:S(2)}) copy-start(f32[512,4]{0,1:T(4,128)} %param.28) | copy-start | bytes 24580
  161.3 1.3 copy-start.13
  161.3 50.7 %all-gather.5.cloned.1.call-start = ((), (), s32[]{:S(2)}) async-start(), calls=%async_computation.4 | async-start | bytes 1310720 | tf_op jit(solution)/shard_map/all_gather | solution.py:444
  162.6 2.9 %copy-start.8 = (bf16[2048,256]{1,0:T(8,128)(2,1)S(1)}, bf16[2048,256]{1,0:T(8,128)(2,1)}, u32[]{:S(2)}) copy-start(bf16[2048,256]{1,0:T(8,128)(2,1)} %param.24) | copy-start | bytes 3145732
  165.5 1.3 copy-start.9
  166.8 1.3 copy-start.10
  168.1 0.8 copy-start.14
  168.1 0.8 copy-start.15
  168.9 2.4 %copy-start.3 = (f32[256]{0:T(256)S(1)}, f32[256]{0:T(256)}, u32[]{:S(2)}) copy-start(f32[256]{0:T(256)} %param.31) | copy-start | bytes 3076
  171.3 1.0 copy-start.4
  172.4 23.8 %copy-start.12 = (bf16[128,512]{1,0:T(8,128)(2,1)S(1)}, bf16[128,512]{1,0:T(8,128)(2,1)}, u32[]{:S(2)}) copy-start(bf16[128,512]{1,0:T(8,128)(2,1)} %param.39) | copy-start | bytes 393220
  199.4 12.7 %copy-start.11 = (bf16[1024,512]{1,0:T(8,128)(2,1)S(1)}, bf16[1024,512]{1,0:T(8,128)(2,1)}, u32[]{:S(2)}) copy-start(bf16[1024,512]{1,0:T(8,128)(2,1)} %param.32) | copy-start | bytes 3145732
Sparse Core Ops, SparseCore 0:
  161.5 21.6 all-gather.6
  196.3 15.6 all-gather.4

commit v2 on v1

--- a/solution.py
+++ b/solution.py
@@ -204,92 +204,163 @@
     )(query_vec, key_vec, value_vec, log_fade, rate_gate, norm_gain.reshape(1, width))
 
 
-def partial_kernel(heads, per_step, ids_ref, query_ref, key_ref, value_ref, out_ref, sum_ref):
-    base = pl.program_id(0) * per_step
+def pack_kernel(capacity, asking_ref, wanted_ref, dots_ref, gain_ref, *refs):
+    *out_refs, held = refs
+    owner = pl.program_id(0)
+    heads = len(out_refs)
+
+    @pl.when(owner == 0)
+    def _():
+        for head in range(heads):
+            span = pl.ds(head * XHEAD, XHEAD)
+            for block in range(held.shape[0]):
+                dots = dots_ref[pl.ds(block * QBLOCK, QBLOCK), span]
+                mean = jnp.mean(dots * dots, axis=-1, keepdims=True)
+                held[block, :, span] = (
+                    dots * lax.rsqrt(mean + 1e-06) * gain_ref[:, span]
+                ).astype(BFLOAT)
+
+    extra = out_refs[0].shape[1] - capacity * QBLOCK
+    row = lax.broadcasted_iota(jnp.int32, (extra, XHEAD), 0)
+    names = jnp.zeros((extra, XHEAD), FLOAT32)
+    for slot in range(capacity):
+        block = asking_ref[owner * capacity + slot]
+        names = jnp.where(row == slot, wanted_ref[owner * capacity + slot].astype(FLOAT32), names)
+        for head in range(heads):
+            out_refs[head][0, pl.ds(slot * QBLOCK, QBLOCK), :] = held[
+                block, :, pl.ds(head * XHEAD, XHEAD)
+            ]
+    for head in range(heads):
+        out_refs[head][0, pl.ds(capacity * QBLOCK, extra), :] = names.astype(BFLOAT)
+
+
+def pack_queries(asking, wanted, dots, score_gain, payload, capacity):
+    rows, width = dots.shape
+    heads = width // XHEAD
+    owners = payload[0]
+    return pl.pallas_call(
+        functools.partial(pack_kernel, capacity),
+        grid_spec=pltpu.PrefetchScalarGridSpec(
+            num_scalar_prefetch=2,
+            grid=(owners,),
+            in_specs=[
+                pl.BlockSpec((rows, width), lambda i, *_: (0, 0)),
+                pl.BlockSpec((1, width), lambda i, *_: (0, 0)),
+            ],
+            out_specs=[pl.BlockSpec((1,) + payload[1:], lambda i, *_: (i, 0, 0))] * heads,
+            scratch_shapes=[pltpu.VMEM((rows // QBLOCK, QBLOCK, width), BFLOAT)],
+        ),
+        out_shape=[jax.ShapeDtypeStruct(payload, BFLOAT)] * heads,
+        compiler_params=pltpu.CompilerParams(dimension_semantics=("arbitrary",)),
+        cost_estimate=pl.CostEstimate(
+            flops=rows * width * 8, bytes_accessed=rows * width * 12, transcendentals=0
+        ),
+    )(asking, wanted, dots, score_gain.reshape(1, width))
+
+
+def partial_kernel(capacity, ids_ref, query_ref, key_ref, value_ref, out_ref):
+    base = pl.program_id(0) * capacity
     length = key_ref.shape[1]
     ones = jnp.ones((8, length), BFLOAT)
-    for slot in range(per_step):
+    extra = out_ref.shape[1] - capacity * QBLOCK
+    row = lax.broadcasted_iota(jnp.int32, (extra, XHEAD), 0)
+    totals = jnp.zeros((extra, XHEAD), FLOAT32)
+    for slot in range(capacity):
         passage = ids_ref[base + slot]
-        for head in range(heads):
-            span = pl.ds(head * XHEAD, XHEAD)
-            scores = raw_dot(
-                query_ref[slot, :, span], key_ref[passage, :, span], ((1,), (1,))
-            ) * XHEAD ** (-0.5)
-            expon = jnp.exp(scores).astype(BFLOAT)
-            out_ref[slot, :, span] = raw_dot(
-                expon, value_ref[passage, :, span], ((1,), (0,))
-            ).astype(BFLOAT)
-            sums = raw_dot(ones, expon, ((1,), (1,)))
-            sum_ref[slot, pl.ds(head, 1), :] = sums[:1]
-
-
-def partial_attention(ids, queries, keys, values):
-    slots, tokens, width = queries.shape
-    heads = width // XHEAD
-    per_step = 4 if slots % 4 == 0 else 2
-    whole = pl.BlockSpec(keys.shape, lambda i, ids: (0, 0, 0))
+        span = pl.ds(slot * QBLOCK, QBLOCK)
+        scores = raw_dot(query_ref[0, span, :], key_ref[passage], ((1,), (1,))) * XHEAD ** (-0.5)
+        expon = jnp.exp(scores).astype(BFLOAT)
+        out_ref[0, span, :] = raw_dot(expon, value_ref[passage], ((1,), (0,))).astype(BFLOAT)
+        sums = raw_dot(ones, expon, ((1,), (1,)))[:1]
+        high = sums.astype(BFLOAT).astype(FLOAT32)
+        middle = (sums - high).astype(BFLOAT).astype(FLOAT32)
+        low = sums - high - middle
+        line = jnp.concatenate(
+            [high, middle, low] + [jnp.zeros_like(low)] * (XHEAD // QBLOCK - 3), axis=1
+        )
+        totals = jnp.where(row == slot, line, totals)
+    out_ref[0, pl.ds(capacity * QBLOCK, extra), :] = totals.astype(BFLOAT)
+
+
+def partial_attention(ids, queries, keys, values, capacity, head):
+    owners, rows, _ = queries.shape
+    whole = pl.BlockSpec(keys.shape[:2] + (XHEAD,), lambda i, ids: (0, 0, head))
+    piece = pl.BlockSpec((1, rows, XHEAD), lambda i, ids: (i, 0, 0))
     return pl.pallas_call(
-        functools.partial(partial_kernel, heads, per_step),
+        functools.partial(partial_kernel, capacity),
         grid_spec=pltpu.PrefetchScalarGridSpec(
             num_scalar_prefetch=1,
-            grid=(slots // per_step,),
-            in_specs=[
-                pl.BlockSpec((per_step, tokens, width), lambda i, ids: (i, 0, 0)),
-                whole,
-                whole,
-            ],
-            out_specs=[
-                pl.BlockSpec((per_step, tokens, width), lambda i, ids: (i, 0, 0)),
-                pl.BlockSpec((per_step, heads, tokens), lambda i, ids: (i, 0, 0)),
-            ],
-        ),
-        out_shape=[
-            jax.ShapeDtypeStruct((slots, tokens, width), BFLOAT),
-            jax.ShapeDtypeStruct((slots, heads, tokens), FLOAT32),
-        ],
+            grid=(owners,),
+            in_specs=[piece, whole, whole],
+            out_specs=piece,
+        ),
+        out_shape=jax.ShapeDtypeStruct(queries.shape, BFLOAT),
         compiler_params=pltpu.CompilerParams(
             dimension_semantics=("arbitrary",), vmem_limit_bytes=32 * 1024 * 1024
         ),
         cost_estimate=pl.CostEstimate(
-            flops=slots * tokens * width * keys.shape[1] * 4,
-            bytes_accessed=slots * tokens * width * 4,
+            flops=owners * rows * XHEAD * keys.shape[1] * 8,
+            bytes_accessed=owners * rows * XHEAD * 4,
             transcendentals=0,
         ),
     )(ids, queries, keys, values)
 
 
-def combine_kernel(heads, where_ref, *refs):
-    *part_refs, scale_ref, out_ref = refs
-    for head in range(heads):
-        span = pl.ds(head * XHEAD, XHEAD)
-        total = part_refs[0][0, :, span].astype(FLOAT32)
-        for part in part_refs[1:]:
-            total = total + part[0, :, span].astype(FLOAT32)
-        out_ref[:, span] = (total * scale_ref[0, :, head : head + 1]).astype(BFLOAT)
-
-
-def combine(where, parts, scale):
-    blocks, per_block = where.shape
-    _, tokens, width = parts.shape
-    heads = width // XHEAD
-
-    def part_spec(place):
-        return pl.BlockSpec(
-            (1, tokens, width), lambda i, where: (where[i * per_block + place], 0, 0)
+def combine_kernel(per_block, capacity, owner_ref, rank_ref, parts_ref, out_ref):
+    blocks = out_ref.shape[0] // QBLOCK
+    extra = parts_ref.shape[1] - capacity * QBLOCK
+    row = lax.broadcasted_iota(jnp.int32, (extra, XHEAD), 0)
+    diagonal = lax.broadcasted_iota(jnp.int32, (QBLOCK, QBLOCK), 0) == lax.broadcasted_iota(
+        jnp.int32, (QBLOCK, QBLOCK), 1
+    )
+    for block in range(blocks):
+        total = jnp.zeros((QBLOCK, XHEAD), FLOAT32)
+        lines = jnp.zeros((extra, XHEAD), FLOAT32)
+        for place in range(per_block):
+            owner = owner_ref[block * per_block + place]
+            rank = rank_ref[block * per_block + place]
+            start = pl.multiple_of(rank * QBLOCK, QBLOCK)
+            total = total + parts_ref[owner, pl.ds(start, QBLOCK), :].astype(FLOAT32)
+            tail = parts_ref[owner, pl.ds(capacity * QBLOCK, extra), :].astype(FLOAT32)
+            lines = lines + jnp.where(row == rank, tail, 0.0)
+        line = jnp.sum(lines, axis=0, keepdims=True)
+        sums = (
+            line[:, :QBLOCK] + line[:, QBLOCK : 2 * QBLOCK] + line[:, 2 * QBLOCK : 3 * QBLOCK]
         )
-
+        column = jnp.sum(jnp.where(diagonal, 1.0 / sums, 0.0), axis=1, keepdims=True)
+        out_ref[pl.ds(block * QBLOCK, QBLOCK), :] = (total * column).astype(BFLOAT)
+
+
+def combine(owner_of, slot_rank, parts, capacity, block_count):
+    per_block = owner_of.shape[0] // block_count
     return pl.pallas_call(
-        functools.partial(combine_kernel, heads),
+        functools.partial(combine_kernel, per_block, capacity),
         grid_spec=pltpu.PrefetchScalarGridSpec(
-            num_scalar_prefetch=1,
-            grid=(blocks,),
-            in_specs=[part_spec(place) for place in range(per_block)]
-            + [pl.BlockSpec((1, tokens, heads), lambda i, where: (i, 0, 0))],
-            out_specs=pl.BlockSpec((tokens, width), lambda i, where: (i, 0)),
-        ),
-        out_shape=jax.ShapeDtypeStruct((blocks * tokens, width), BFLOAT),
+            num_scalar_prefetch=2,
+            grid=(1,),
+            in_specs=[pl.BlockSpec(parts.shape, lambda i, *_: (0, 0, 0))],
+            out_specs=pl.BlockSpec((block_count * QBLOCK, XHEAD), lambda i, *_: (0, 0)),
+        ),
+        out_shape=jax.ShapeDtypeStruct((block_count * QBLOCK, XHEAD), BFLOAT),
         compiler_params=pltpu.CompilerParams(dimension_semantics=("arbitrary",)),
-    )(where.reshape(-1), *([parts] * per_block), scale)
+        cost_estimate=pl.CostEstimate(
+            flops=parts.size * 4, bytes_accessed=parts.size * 3, transcendentals=0
+        ),
+    )(owner_of, slot_rank, parts)
+
+
+def spread_product(piece, weights):
+    count = lax.axis_size("tp")
+    me = lax.axis_index("tp")
+    total = None
+    for shift in range(count):
+        moved = piece
+        if shift:
+            moved = lax.ppermute(piece, "tp", [(i, (i ^ shift)) for i in range(count)])
+        rows = lax.dynamic_index_in_dim(weights, me ^ shift, 0, keepdims=False)
+        term = jnp.dot(moved, rows, preferred_element_type=FLOAT32)
+        total = term if total is None else total + term
+    return total
 
 
 def mixer(
@@ -375,18 +446,18 @@
     chosen = to_owner[:, :, None] & to_slot[:, None, :]
     wanted = jnp.sum(jnp.where(chosen, local_idx[:, None, None], 0), axis=0)
     asking = jnp.sum(jnp.where(chosen, (slot_order // per_block)[:, None, None], 0), axis=0)
-    where_from = owner_of * capacity + slot_rank
-
-    served = lax.all_to_all(wanted, "st", split_axis=0, concat_axis=0, tiled=True).reshape(-1)
-    queries = (
-        head_norm(jnp.dot(tokens, cross_query, preferred_element_type=FLOAT32), XHEAD)
-        * score_gain
-    )
-    queries = queries.astype(BFLOAT).reshape(block_count, QBLOCK, cross_width)
-    outgoing = queries[asking.reshape(-1)].reshape(
-        owner_count, capacity, QBLOCK, cross_width
-    )
-    incoming = lax.all_to_all(outgoing, "st", split_axis=0, concat_axis=0, tiled=True)
+
+    extra = -(-capacity // 8) * 8
+    payload = (owner_count, capacity * QBLOCK + extra, XHEAD)
+
+    def exchange(values):
+        return lax.all_to_all(values, "st", split_axis=0, concat_axis=0, tiled=True)
+
+    dots = jnp.dot(tokens, cross_query, preferred_element_type=FLOAT32)
+    outgoing = pack_queries(
+        asking.reshape(-1), wanted.reshape(-1), dots, score_gain, payload, capacity
+    )
+    incoming = [exchange(outgoing[head]) for head in range(head_count)]
     flat_rows = store.reshape(-1, model_width)
     keyed = head_norm(
         jnp.dot(flat_rows, passage_key, preferred_element_type=FLOAT32), XHEAD
@@ -394,26 +465,13 @@
     valued = jnp.dot(flat_rows, passage_value, preferred_element_type=FLOAT32).astype(BFLOAT)
     keyed = keyed.reshape(pass_dev, passage_len, cross_width)
     valued = valued.reshape(pass_dev, passage_len, cross_width)
-    parts, sums = partial_attention(
-        served,
-        incoming.reshape(owner_count * capacity, QBLOCK, cross_width),
-        keyed,
-        valued,
-    )
-    sums = lax.all_to_all(
-        sums.reshape(owner_count, capacity, head_count, QBLOCK),
-        "st",
-        split_axis=0,
-        concat_axis=0,
-        tiled=True,
-    )
-    parts = lax.all_to_all(
-        parts.reshape(owner_count, capacity, QBLOCK, cross_width),
-        "st",
-        split_axis=0,
-        concat_axis=0,
-        tiled=True,
-    )
+    parts = []
+    for head in range(head_count):
+        if head == 0:
+            names = incoming[0][:, capacity * QBLOCK : capacity * QBLOCK + capacity, 0]
+            served = names.astype(jnp.int32).reshape(-1)
+        part = partial_attention(served, incoming[head], keyed, valued, capacity, head)
+        parts.append(exchange(part))
     mixer_heads = mixer(
         tokens,
         mix_query,
@@ -427,32 +485,23 @@
         rate_upper_map,
         norm_gain,
     )
-    sums = sums.reshape(owner_count * capacity, head_count, QBLOCK)[where_from]
-    sums = jnp.sum(sums.reshape(block_count, per_block, head_count, QBLOCK), axis=1)
-    scale = (1.0 / sums).transpose(0, 2, 1)
-    attended = combine(
-        where_from.reshape(block_count, per_block),
-        parts.reshape(owner_count * capacity, QBLOCK, cross_width),
-        scale,
-    )
     shard_total = lax.axis_size("tp")
     out_cols = mix_out.shape[1]
-    mix_rows = mix_out.reshape(shard_total, -1, out_cols)
-    cross_rows = cross_out.reshape(shard_total, -1, out_cols)
-    mixer_part = jnp.einsum(
-        "ntc,ncd->td",
-        lax.all_gather(mixer_heads[None], "tp", axis=0, tiled=True),
-        mix_rows,
-        preferred_element_type=FLOAT32,
+    mixer_part = lax.optimization_barrier(
+        spread_product(mixer_heads, mix_out.reshape(shard_total, -1, out_cols))
     )
     gate_low = jnp.dot(tokens, gate_down, preferred_element_type=FLOAT32).astype(BFLOAT)
-    gate_open = jax.nn.sigmoid(jnp.dot(gate_low, gate_up, preferred_element_type=FLOAT32))
-    cross_part = jnp.einsum(
-        "ntc,ncd->td",
-        lax.all_gather(attended[None], "tp", axis=0, tiled=True),
-        cross_rows,
-        preferred_element_type=FLOAT32,
-    )
+    gate_open = lax.optimization_barrier(
+        jax.nn.sigmoid(jnp.dot(gate_low, gate_up, preferred_element_type=FLOAT32))
+    )
+    cross_rows = cross_out.reshape(shard_total, head_count, XHEAD, out_cols)
+    cross_part = None
+    for head in range(head_count):
+        attended = combine(owner_of, slot_rank, parts[head], capacity, block_count)
+        term = spread_product(attended, cross_rows[:, head])
+        if head < head_count - 1:
+            term = lax.optimization_barrier(term)
+        cross_part = term if cross_part is None else cross_part + term
     return (mixer_part + gate_open * cross_part).astype(BFLOAT)
 
 

time: 223 us -> 196 us (0.88)
  waiting for transfers between devices: 75.2 us -> 52.1 us
  between operations: 13.7 us -> 0.36 us
  blocking collectives: 10 us -> 0 us
  starting transfers between devices: 17.9 us -> 26.9 us
  matrix products: 35.3 us -> 40.8 us
  Pallas kernels: 39.7 us -> 44.7 us
    all_to_all x3 -> x4, waiting for transfers between devices: 67.5 us -> 33.8 us  [exchange(): return lax.all_to_all(values, 'st', split_axis=0, concat_axis=0, tiled=True)]
    ppermute x0 -> x9, waiting for transfers between devices: none -> 18.3 us  [spread_product(): moved = lax.ppermute(piece, 'tp', [(i, i ^ shift) for i in range(count)])]
    all_to_all x1 -> x0, blocking collectives: 10 us -> none  [layer(): lax.all_to_all(sums.reshape(owner_count, capacity, head_count, QBLOCK), '...]
    all_gather x2 -> x0, waiting for transfers between devices: 7.73 us -> none  [the longest x1 7.73 us: layer(): lax.all_gather(mixer_heads[None], 'tp', axis=0, tiled=True)]
    ppermute x0 -> x9, starting transfers between devices: none -> 6.54 us  [spread_product(): moved = lax.ppermute(piece, 'tp', [(i, i ^ shift) for i in range(count)])]
    pallas_call x2 -> x5, Pallas kernels: 15.9 us -> 21.5 us  [the longest x2 10.6 us: partial_attention(): pl.pallas_call(functools.partial(partial_kernel, capacity), grid_spec=plt...]
    slice x0 -> x1, local copies, waits for them, and re-layouts: none -> 3.14 us  [layer(): term = spread_product(attended, cross_rows[:, head])]
    dot_general x3, matrix products: 2.12 us -> 4.86 us  [project(): jnp.dot(tokens, weight, preferred_element_type=FLOAT32).astype(BFLOAT)]
  transfers between devices with their start and end apart: 5 -> 13, of which waited for: 3 -> 6; matrix products, arithmetic and copies ran while one was open for 24% -> 27% of each run, Pallas kernels for 11% -> 17%
where the time goes in v2:
time: 196 us; the launch traced here: 195 us
  waiting for transfers between devices  52.1 us (27%)
  Pallas kernels  44.7 us (23%)
  matrix products  40.8 us (21%)
  starting transfers between devices  26.9 us (14%)
  local copies, waits for them, and re-layouts  25.7 us (13%)
  other arithmetic  4.25 us (2%)
    all_to_all x4, waiting for transfers between devices, exchange(): return lax.all_to_all(values, 'st', split_axis=0, concat_axis=0, tiled=True)  33.8 us
    pallas_call x1, Pallas kernels, recurrence(): pl.pallas_call(functools.partial(mixer_kernel, heads, blocks), grid=(rows...  23.2 us
    all_to_all x4, starting transfers between devices, exchange(): return lax.all_to_all(values, 'st', split_axis=0, concat_axis=0, tiled=True)  20.3 us
    ppermute x9, waiting for transfers between devices, spread_product(): moved = lax.ppermute(piece, 'tp', [(i, i ^ shift) for i in range(count)])  18.3 us
    pallas_call x2, Pallas kernels, partial_attention(): pl.pallas_call(functools.partial(partial_kernel, capacity), grid_spec=plt...  10.6 us
    dot_general x12, matrix products, spread_product(): term = jnp.dot(moved, rows, preferred_element_type=FLOAT32)  10.5 us
    unnamed x50, local copies, waits for them, and re-layouts  7.96 us
    dot_general x1, matrix products, layer(): jnp.dot(flat_rows, passage_value, preferred_element_type=FLOAT32)  6.67 us
  transfers between devices with their start and end apart: 13, of which 6 were waited for; matrix products, arithmetic and copies ran while one was open for 27% of the time, Pallas kernels for 17%

profile of v2, /device:TPU:0, one launch (start us, length us, event | category | flops | bytes accessed | tf_op | source)
XLA Modules:
  0.0 194.9 jit_solution(2753133236096190792)
XLA Ops:
  3.9 3.8 %fusion.62.dots_ref = f32[512,512]{1,0:T(8,128)} fusion(bf16[512,2048]{1,0:T(8,128)(2,1)S(1)} %copy-done, bf16[2048,512]{1,0:T(8,128)(2,1)} %param.33), kind=kOutput, calls=%fused_computation.99 | convolution fusion | flops 1073741824 | bytes 5242880 | tf_op jit(solution)/shard_map/dot_general | solution.py:456
  7.7 5.2 %shard_map.200 = (bf16[8,264,256]{2,1,0:T(8,128)(2,1)}, bf16[8,264,256]{2,1,0:T(8,128)(2,1)}) custom-call(s32[32]{0:T(128)} %reshape.169.asking_ref, s32[32]{0:T(128)} %reshape.170.wanted_ref, f32[512,512]{1,0:T(8,128)} %fusion.62.dots_ref, f32[1,512]{1,0:T(1,128)} %bitcast.91), custom_call_target="tpu_custom_call" | custom-call | flops 2097152 | bytes 3145728 | tf_op jit(solution)/shard_map/pallas_call | solution.py:241
  12.9 7.3 %all-to-all-start = ((bf16[8,264,256]{2,1,0:T(8,128)(2,1)}), bf16[8,264,256]{2,1,0:T(8,128)(2,1)S(1)}, u32[]{:S(2)}, u32[]{:S(2)}) async-start(bf16[8,264,256]{2,1,0:T(8,128)(2,1)} %get-tuple-element.7), calls=%async_computation | async-start | bytes 2162688 | tf_op jit(solution)/shard_map/all_to_all | solution.py:454
  20.2 3.9 %copy.42 = bf16[512,2048]{1,0:T(8,128)(2,1)} copy(bf16[512,2048]{0,1:T(8,128)(2,1)} %bitcast.83) | data formatting | bytes 4194304 | tf_op jit(solution)/shard_map/dot_general | solution.py:463
  24.1 22.5 %all-to-all-done.query_ref = bf16[8,264,256]{2,1,0:T(8,128)(2,1)S(1)} async-done(((bf16[8,264,256]{2,1,0:T(8,128)(2,1)}), bf16[8,264,256]{2,1,0:T(8,128)(2,1)S(1)}, u32[]{:S(2)}, u32[]{:S(2)}) %all-to-all-start) | async-done | bytes 1081376 | tf_op jit(solution)/shard_map/all_to_all | solution.py:454
  46.7 4.2 %all-to-all-start.2 = ((bf16[8,264,256]{2,1,0:T(8,128)(2,1)}), bf16[8,264,256]{2,1,0:T(8,128)(2,1)}, u32[]{:S(2)}, u32[]{:S(2)}) async-start(bf16[8,264,256]{2,1,0:T(8,128)(2,1)} %get-tuple-element.8), calls=%async_computation.2 | async-start | bytes 2162688 | tf_op jit(solution)/shard_map/all_to_all | solution.py:454
  50.9 6.0 %multiply_reduce_fusion = (f32[1152,2]{0,1:T(2,128)S(1)}, f32[1152,2,256]{0,2,1:T(8,128)S(1)}) fusion(bf16[1152,2048,1]{1,0,2:T(8,128)(2,1)} %bitcast.92, bf16[2,256,2048]{2,1,0:T(8,128)(2,1)} %bitcast.85), kind=kOutput, calls=%fused_computation.2 | convolution fusion | flops 2417096448 | bytes 9184256 | tf_op jit(solution)/shard_map/dot_general | solution.py:463
  57.1 2.7 %copy.41 = bf16[1152,2,256]{2,1,0:T(2,128)(2,1)} copy(bf16[1152,2,256]{0,2,1:T(8,128)(2,1)S(1)} %multiply_convert_fusion) | data formatting | bytes 2359296 | tf_op jit(solution)/shard_map/convert_element_type | solution.py:464
  59.7 3.1 %convert_element_type.51.key_ref = bf16[12,96,512]{2,1,0:T(8,128)(2,1)S(1)} reshape(bf16[1152,2,256]{2,1,0:T(2,128)(2,1)} %copy.41) | data formatting | bytes 2359296 | tf_op jit(solution)/shard_map/convert_element_type | solution.py:464
  62.9 6.7 %convolution_convert_fusion = bf16[1152,512]{1,0:T(8,128)(2,1)} fusion(bf16[1152,2048]{1,0:T(8,128)(2,1)} %bitcast.93, bf16[2048,512]{1,0:T(8,128)(2,1)} %param.36), kind=kOutput, calls=%fused_computation | convolution fusion | flops 2416508928 | bytes 7995392 | tf_op jit(solution)/shard_map/dot_general | solution.py:465
  70.6 6.6 %all-to-all-done.2.query_ref = bf16[8,264,256]{2,1,0:T(8,128)(2,1)} async-done(((bf16[8,264,256]{2,1,0:T(8,128)(2,1)}), bf16[8,264,256]{2,1,0:T(8,128)(2,1)}, u32[]{:S(2)}, u32[]{:S(2)}) %all-to-all-start.2) | async-done | bytes 1081376 | tf_op jit(solution)/shard_map/all_to_all | solution.py:454
  77.2 1.3 copy-done.1
  78.5 6.4 %shard_map.203 = bf16[8,264,256]{2,1,0:T(8,128)(2,1)S(1)} custom-call(s32[32]{0:T(128)S(1)} %reshape.175.ids_ref, bf16[8,264,256]{2,1,0:T(8,128)(2,1)} %all-to-all-done.2.query_ref, bf16[12,96,512]{2,1,0:T(8,128)(2,1)S(1)} %convert_element_type.51.key_ref, bf16[12,96,512]{2,1,0:T(8,128)(2,1)S(1)} %bitcast.80), custom_call_target="tpu_custom_call" | custom-call | flops 415236096 | bytes 2162688 | tf_op jit(solution)/shard_map/pallas_call | solution.py:289
  84.9 1.0 copy-done.6
  85.9 4.5 %all-to-all-start.3 = ((bf16[8,264,256]{2,1,0:T(8,128)(2,1)}), bf16[8,264,256]{2,1,0:T(8,128)(2,1)}, u32[]{:S(2)}, u32[]{:S(2)}) async-start(bf16[8,264,256]{2,1,0:T(8,128)(2,1)} %copy-done.6), calls=%async_computation.3 | async-start | bytes 2162688 | tf_op jit(solution)/shard_map/all_to_all | solution.py:454
  91.3 2.0 %copy.34 = f32[512,256]{1,0:T(8,128)} copy(f32[512,256]{0,1:T(8,128)} %bitcast.86) | data formatting | bytes 1048576 | tf_op jit(solution)/shard_map/reshape | solution.py:394
  93.4 2.6 %fusion.8.gate_ref = f32[512,256]{1,0:T(8,128)} fusion(bf16[64,256]{1,0:T(8,128)(2,1)} %param.30, bf16[512,2048]{1,0:T(8,128)(2,1)S(1)} %copy-done, bf16[2048,64]{0,1:T(8,128)(2,1)S(1)} %copy-done.22), kind=kOutput, calls=%fused_computation.20 | convolution fusion | flops 151420928 | bytes 2916352 | tf_op jit(solution)/shard_map/dot_general | solution.py:398
  96.0 2.0 %convolution_convert_fusion.1.value_ref = bf16[512,256]{1,0:T(8,128)(2,1)S(1)} fusion(bf16[512,2048]{1,0:T(8,128)(2,1)S(1)} %copy-done, bf16[2048,256]{1,0:T(8,128)(2,1)} %param.24), kind=kOutput, calls=%fused_computation.24 | convolution fusion | flops 537001984 | bytes 3407872 | tf_op jit(solution)/shard_map/dot_general | solution.py:383
  98.0 1.4 convolution_convert_fusion.2.key_ref
  99.5 1.4 convolution_convert_fusion.3.query_ref
  100.9 3.2 %fusion.15.fade_ref = f32[512,256]{1,0:T(8,128)} fusion(f32[512,256]{1,0:T(8,128)} %copy.34, bf16[64,256]{1,0:T(8,128)(2,1)} %param.26, bf16[512,2048]{1,0:T(8,128)(2,1)S(1)} %copy-done, bf16[2048,64]{0,1:T(8,128)(2,1)} %param.25, f32[256]{0:T(256)S(1)} %copy-done.24), kind=kOutput, calls=%fused_computation.35 | convolution fusion | flops 152600576 | bytes 3441664 | tf_op jit(solution)/shard_map/dot_general | solution.py:393
  104.1 1.3 copy-done.2
  105.4 1.2 copy-done.4
  106.6 4.2 %shard_map.201 = bf16[8,264,256]{2,1,0:T(8,128)(2,1)S(1)} custom-call(s32[32]{0:T(128)S(1)} %reshape.175.ids_ref, bf16[8,264,256]{2,1,0:T(8,128)(2,1)S(1)} %copy-done.4, bf16[12,96,512]{2,1,0:T(8,128)(2,1)S(1)} %convert_element_type.51.key_ref, bf16[12,96,512]{2,1,0:T(8,128)(2,1)S(1)} %bitcast.81), custom_call_target="tpu_custom_call" | custom-call | flops 415236096 | bytes 2162688 | tf_op jit(solution)/shard_map/pallas_call | solution.py:289
  110.8 1.0 copy-done.5
  111.8 4.7 %all-to-all-done.3.parts_ref = bf16[8,264,256]{2,1,0:T(8,128)(2,1)} async-done(((bf16[8,264,256]{2,1,0:T(8,128)(2,1)}), bf16[8,264,256]{2,1,0:T(8,128)(2,1)}, u32[]{:S(2)}, u32[]{:S(2)}) %all-to-all-start.3) | async-done | bytes 1081376 | tf_op jit(solution)/shard_map/all_to_all | solution.py:454
  116.5 4.3 %all-to-all-start.1 = ((bf16[8,264,256]{2,1,0:T(8,128)(2,1)}), bf16[8,264,256]{2,1,0:T(8,128)(2,1)}, u32[]{:S(2)}, u32[]{:S(2)}) async-start(bf16[8,264,256]{2,1,0:T(8,128)(2,1)} %copy-done.5), calls=%async_computation.1 | async-start | bytes 2162688 | tf_op jit(solution)/shard_map/all_to_all | solution.py:454
  120.8 1.0 copy-done.10
  121.8 1.0 copy-done.11
  122.9 23.2 %shard_map.199 = bf16[512,256]{1,0:T(8,128)(2,1)S(1)} custom-call(bf16[512,256]{1,0:T(8,128)(2,1)S(1)} %copy-done.9, bf16[512,256]{1,0:T(8,128)(2,1)S(1)} %copy-done.8, bf16[512,256]{1,0:T(8,128)(2,1)S(1)} %convolution_convert_fusion.1.value_ref, f32[512,256]{1,0:T(8,128)S(1)} %copy-done.10, f32[512,256]{1,0:T(8,128)S(1)} %copy-done.11, f32[1,256]{1,0:T(1,128)S(1)} %bitcast.82), custom_call_target="tpu_custom_call" | custom-call | flops 5242880000 | bytes 2097152 | tf_op jit(solution)/shard_map/pallas_call | solution.py:191
  146.1 1.6 collective-permute-start.2
  148.3 3.2 %fusion.2 = f32[512,512]{1,0:T(8,128)} fusion(bf16[128,512]{1,0:T(8,128)(2,1)S(1)} %copy-done.23, bf16[512,2048]{1,0:T(8,128)(2,1)S(1)} %copy-done, bf16[2048,128]{1,0:T(8,128)(2,1)} %param.38), kind=kOutput, calls=%fused_computation.7 | convolution fusion | flops 336396288 | bytes 3801088 | tf_op jit(solution)/shard_map/dot_general | solution.py:495
  151.4 3.1 %fusion.61 = (bf16[4,1,256,512]{3,2,1,0:T(8,128)(2,1)}, bf16[4,1,256,512]{3,2,1,0:T(8,128)(2,1)}) fusion(bf16[4,2,256,512]{3,2,1,0:T(8,128)(2,1)} %bitcast.84), kind=kLoop, calls=%fused_computation.98 | loop fusion | bytes 4194304 | tf_op jit(solution)/shard_map/slice | solution.py:501
  154.9 1.2 convolution_add_fusion.5
  156.1 1.3 fusion.28
  157.4 3.1 %collective-permute-done.1 = bf16[512,256]{1,0:T(8,128)(2,1)} collective-permute-done((bf16[512,256]{1,0:T(8,128)(2,1)S(1)}, bf16[512,256]{1,0:T(8,128)(2,1)}, u32[]{:S(2)}, u32[]{:S(2)}) %collective-permute-start.1) | collective-permute-done | bytes 262176 | tf_op jit(solution)/shard_map/ppermute | solution.py:359
  160.5 1.3 fusion.5
  161.9 2.9 %shard_map.204 = bf16[512,256]{1,0:T(8,128)(2,1)} custom-call(s32[32]{0:T(128)} %copy-done.18, s32[32]{0:T(128)} %copy-done.19, bf16[8,264,256]{2,1,0:T(8,128)(2,1)} %all-to-all-done.3.parts_ref), custom_call_target="tpu_custom_call" | custom-call | flops 2162688 | bytes 1622016 | tf_op jit(solution)/shard_map/pallas_call | solution.py:336
  164.8 1.6 collective-permute-start.8
  166.9 2.9 %shard_map.202 = bf16[512,256]{1,0:T(8,128)(2,1)} custom-call(s32[32]{0:T(128)} %copy-done.18, s32[32]{0:T(128)} %copy-done.19, bf16[8,264,256]{2,1,0:T(8,128)(2,1)} %all-to-all-done.1.parts_ref), custom_call_target="tpu_custom_call" | custom-call | flops 2162688 | bytes 1622016 | tf_op jit(solution)/shard_map/pallas_call | solution.py:336
  169.8 1.6 collective-permute-start.5
  171.4 1.3 fusion.20
  172.7 1.3 fusion.26
  175.0 9.7 %collective-permute-done.5 = bf16[512,256]{1,0:T(8,128)(2,1)S(1)} collective-permute-done((bf16[512,256]{1,0:T(8,128)(2,1)}, bf16[512,256]{1,0:T(8,128)(2,1)S(1)}, u32[]{:S(2)}, u32[]{:S(2)}) %collective-permute-start.5) | collective-permute-done | bytes 262176 | tf_op jit(solution)/shard_map/ppermute | solution.py:359
  184.9 5.5 %collective-permute-done.4 = bf16[512,256]{1,0:T(8,128)(2,1)S(1)} collective-permute-done((bf16[512,256]{1,0:T(8,128)(2,1)S(1)}, bf16[512,256]{1,0:T(8,128)(2,1)S(1)}, u32[]{:S(2)}, u32[]{:S(2)}) %collective-permute-start.4) | collective-permute-done | bytes 262176 | tf_op jit(solution)/shard_map/ppermute | solution.py:359
  190.7 1.3 convolution_add_fusion.1
  192.3 1.3 fusion.3
  193.7 1.2 add_convert_fusion
  (83 shorter events, 9.2 us)
Async XLA Ops:
  0.0 3.9 %copy-start = (bf16[512,2048]{1,0:T(8,128)(2,1)S(1)}, bf16[512,2048]{1,0:T(8,128)(2,1)}, u32[]{:S(2)}) copy-start(bf16[512,2048]{1,0:T(8,128)(2,1)} %param.21) | copy-start | bytes 6291460
  2.1 5.7 %copy-start.18 = (s32[32]{0:T(128)}, s32[32]{0:T(128)S(1)}, u32[]{:S(2)}) copy-start(s32[32]{0:T(128)S(1)} %get-tuple-element.16.owner_ref) | copy-start | bytes 388
  2.2 5.5 %copy-start.19 = (s32[32]{0:T(128)}, s32[32]{0:T(128)S(1)}, u32[]{:S(2)}) copy-start(s32[32]{0:T(128)S(1)} %convert_reduce_fusion.1.rank_ref) | copy-start | bytes 388
  12.9 33.8 %all-to-all-start = ((bf16[8,264,256]{2,1,0:T(8,128)(2,1)}), bf16[8,264,256]{2,1,0:T(8,128)(2,1)S(1)}, u32[]{:S(2)}, u32[]{:S(2)}) async-start(bf16[8,264,256]{2,1,0:T(8,128)(2,1)} %get-tuple-element.7), calls=%async_computation | async-start | bytes 2162688 | tf_op jit(solution)/shard_map/all_to_all | solution.py:454
  46.7 10.2 %copy-start.3 = (bf16[8,264,256]{2,1,0:T(8,128)(2,1)}, bf16[8,264,256]{2,1,0:T(8,128)(2,1)S(1)}, u32[]{:S(2)}) copy-start(bf16[8,264,256]{2,1,0:T(8,128)(2,1)S(1)} %all-to-all-done.query_ref) | copy-start | bytes 3244036
  46.7 30.5 %all-to-all-start.2 = ((bf16[8,264,256]{2,1,0:T(8,128)(2,1)}), bf16[8,264,256]{2,1,0:T(8,128)(2,1)}, u32[]{:S(2)}, u32[]{:S(2)}) async-start(bf16[8,264,256]{2,1,0:T(8,128)(2,1)} %get-tuple-element.8), calls=%async_computation.2 | async-start | bytes 2162688 | tf_op jit(solution)/shard_map/all_to_all | solution.py:454
  77.2 1.3 copy-start.1
  84.9 1.0 copy-start.6
  85.9 4.6 %copy-start.17 = (f32[512,4]{0,1:T(4,128)S(1)}, f32[512,4]{0,1:T(4,128)}, u32[]{:S(2)}) copy-start(f32[512,4]{0,1:T(4,128)} %param.28) | copy-start | bytes 24580
  85.9 7.5 %copy-start.22 = (bf16[2048,64]{0,1:T(8,128)(2,1)S(1)}, bf16[2048,64]{0,1:T(8,128)(2,1)}, u32[]{:S(2)}) copy-start(bf16[2048,64]{0,1:T(8,128)(2,1)} %param.29) | copy-start | bytes 786436
  85.9 30.6 %all-to-all-start.3 = ((bf16[8,264,256]{2,1,0:T(8,128)(2,1)}), bf16[8,264,256]{2,1,0:T(8,128)(2,1)}, u32[]{:S(2)}, u32[]{:S(2)}) async-start(bf16[8,264,256]{2,1,0:T(8,128)(2,1)} %copy-done.6), calls=%async_computation.3 | async-start | bytes 2162688 | tf_op jit(solution)/shard_map/all_to_all | solution.py:454
  96.0 2.0 %copy-start.20 = (bf16[2048,256]{1,0:T(8,128)(2,1)S(1)}, bf16[2048,256]{1,0:T(8,128)(2,1)}, u32[]{:S(2)}) copy-start(bf16[2048,256]{1,0:T(8,128)(2,1)} %param.23) | copy-start | bytes 3145732
  98.0 1.4 copy-start.21
  99.5 1.4 copy-start.24
  104.1 1.3 copy-start.2
  105.4 1.2 copy-start.4
  110.8 1.0 copy-start.5
  111.8 8.9 %copy-start.7 = (f32[256]{0:T(256)S(1)}, f32[256]{0:T(256)}, u32[]{:S(2)}) copy-start(f32[256]{0:T(256)} %param.31) | copy-start | bytes 3076
  111.8 9.0 %copy-start.8 = (bf16[512,256]{1,0:T(8,128)(2,1)S(1)}, bf16[512,256]{1,0:T(8,128)(2,1)}, u32[]{:S(2)}) copy-start(bf16[512,256]{1,0:T(8,128)(2,1)} %convolution_convert_fusion.2.key_ref) | copy-start | bytes 786436
  111.8 9.0 %copy-start.9 = (bf16[512,256]{1,0:T(8,128)(2,1)S(1)}, bf16[512,256]{1,0:T(8,128)(2,1)}, u32[]{:S(2)}) copy-start(bf16[512,256]{1,0:T(8,128)(2,1)} %convolution_convert_fusion.3.query_ref) | copy-start | bytes 786436
  116.5 50.4 %all-to-all-start.1 = ((bf16[8,264,256]{2,1,0:T(8,128)(2,1)}), bf16[8,264,256]{2,1,0:T(8,128)(2,1)}, u32[]{:S(2)}, u32[]{:S(2)}) async-start(bf16[8,264,256]{2,1,0:T(8,128)(2,1)} %copy-done.5), calls=%async_computation.1 | async-start | bytes 2162688 | tf_op jit(solution)/shard_map/all_to_all | solution.py:454
  120.8 1.0 copy-start.10
  121.8 1.0 copy-start.11
  122.9 25.4 %copy-start.23 = (bf16[128,512]{1,0:T(8,128)(2,1)S(1)}, bf16[128,512]{1,0:T(8,128)(2,1)}, u32[]{:S(2)}) copy-start(bf16[128,512]{1,0:T(8,128)(2,1)} %param.39) | copy-start | bytes 393220
  146.1 8.8 %collective-permute-start = (bf16[512,256]{1,0:T(8,128)(2,1)S(1)}, bf16[512,256]{1,0:T(8,128)(2,1)}, u32[]{:S(2)}, u32[]{:S(2)}) collective-permute-start(bf16[512,256]{1,0:T(8,128)(2,1)S(1)} %shard_map.199), channel_id=1, source_target_pairs={{0,1},{1,0},{2,3},{3,2},{4,5},{5,4},{6,7},{7,6},{8,9},{9,8},{10,11... | collective-permute-start | bytes 786440 | tf_op jit(solution)/shard_map/ppermute | solution.py:359
  146.1 10.0 %collective-permute-start.2 = (bf16[512,256]{1,0:T(8,128)(2,1)S(1)}, bf16[512,256]{1,0:T(8,128)(2,1)}, u32[]{:S(2)}, u32[]{:S(2)}) collective-permute-start(bf16[512,256]{1,0:T(8,128)(2,1)S(1)} %shard_map.199), channel_id=1, source_target_pairs={{0,3},{1,2},{2,1},{3,0},{4,7},{5,6},{6,5},{7,4},{8,11},{9,10},{10,... | collective-permute-start | bytes 786440 | tf_op jit(solution)/shard_map/ppermute | solution.py:359
  147.8 12.8 %collective-permute-start.1 = (bf16[512,256]{1,0:T(8,128)(2,1)S(1)}, bf16[512,256]{1,0:T(8,128)(2,1)}, u32[]{:S(2)}, u32[]{:S(2)}) collective-permute-start(bf16[512,256]{1,0:T(8,128)(2,1)S(1)} %shard_map.199), channel_id=1, source_target_pairs={{0,2},{1,3},{2,0},{3,1},{4,6},{5,7},{6,4},{7,5},{8,10},{9,11},{10,... | collective-permute-start | bytes 786440 | tf_op jit(solution)/shard_map/ppermute | solution.py:359
  151.4 3.1 %copy-start.16 = (bf16[1024,512]{1,0:T(8,128)(2,1)S(1)}, bf16[1024,512]{1,0:T(8,128)(2,1)}, u32[]{:S(2)}) copy-start(bf16[1024,512]{1,0:T(8,128)(2,1)} %param.32) | copy-start | bytes 3145732
  164.8 26.0 %collective-permute-start.6 = (bf16[512,256]{1,0:T(8,128)(2,1)}, bf16[512,256]{1,0:T(8,128)(2,1)}, u32[]{:S(2)}, u32[]{:S(2)}) collective-permute-start(bf16[512,256]{1,0:T(8,128)(2,1)} %shard_map.204), channel_id=1, source_target_pairs={{0,1},{1,0},{2,3},{3,2},{4,5},{5,4},{6,7},{7,6},{8,9},{9,8},{10,11... | collective-permute-start | bytes 786440 | tf_op jit(solution)/shard_map/ppermute | solution.py:359
  164.8 27.3 %collective-permute-start.8 = (bf16[512,256]{1,0:T(8,128)(2,1)}, bf16[512,256]{1,0:T(8,128)(2,1)S(1)}, u32[]{:S(2)}, u32[]{:S(2)}) collective-permute-start(bf16[512,256]{1,0:T(8,128)(2,1)} %shard_map.204), channel_id=1, source_target_pairs={{0,3},{1,2},{2,1},{3,0},{4,7},{5,6},{6,5},{7,4},{8,11},{9,10},{10,... | collective-permute-start | bytes 786440 | tf_op jit(solution)/shard_map/ppermute | solution.py:359
  166.4 25.9 %collective-permute-start.7 = (bf16[512,256]{1,0:T(8,128)(2,1)}, bf16[512,256]{1,0:T(8,128)(2,1)}, u32[]{:S(2)}, u32[]{:S(2)}) collective-permute-start(bf16[512,256]{1,0:T(8,128)(2,1)} %shard_map.204), channel_id=1, source_target_pairs={{0,2},{1,3},{2,0},{3,1},{4,6},{5,7},{6,4},{7,5},{8,10},{9,11},{10,... | collective-permute-start | bytes 786440 | tf_op jit(solution)/shard_map/ppermute | solution.py:359
  169.8 4.3 %copy-start.15 = (bf16[512,256]{1,0:T(8,128)(2,1)S(1)}, bf16[512,256]{1,0:T(8,128)(2,1)}, u32[]{:S(2)}) copy-start(bf16[512,256]{1,0:T(8,128)(2,1)} %shard_map.202) | copy-start | bytes 786436
  169.8 4.9 %copy-start.13 = (bf16[4,1,256,512]{3,2,1,0:T(8,128)(2,1)S(1)}, bf16[4,1,256,512]{3,2,1,0:T(8,128)(2,1)}, u32[]{:S(2)}) copy-start(bf16[4,1,256,512]{3,2,1,0:T(8,128)(2,1)} %get-tuple-element.12) | copy-start | bytes 3145732
  169.8 4.3 %collective-permute-start.3 = (bf16[512,256]{1,0:T(8,128)(2,1)}, bf16[512,256]{1,0:T(8,128)(2,1)S(1)}, u32[]{:S(2)}, u32[]{:S(2)}) collective-permute-start(bf16[512,256]{1,0:T(8,128)(2,1)} %shard_map.202), channel_id=1, source_target_pairs={{0,1},{1,0},{2,3},{3,2},{4,5},{5,4},{6,7},{7,6},{8,9},{9,8},{10,11... | collective-permute-start | bytes 786440 | tf_op jit(solution)/shard_map/ppermute | solution.py:359
  169.8 14.9 %collective-permute-start.5 = (bf16[512,256]{1,0:T(8,128)(2,1)}, bf16[512,256]{1,0:T(8,128)(2,1)S(1)}, u32[]{:S(2)}, u32[]{:S(2)}) collective-permute-start(bf16[512,256]{1,0:T(8,128)(2,1)} %shard_map.202), channel_id=1, source_target_pairs={{0,3},{1,2},{2,1},{3,0},{4,7},{5,6},{6,5},{7,4},{8,11},{9,10},{10,... | collective-permute-start | bytes 786440 | tf_op jit(solution)/shard_map/ppermute | solution.py:359
  174.1 16.3 %collective-permute-start.4 = (bf16[512,256]{1,0:T(8,128)(2,1)S(1)}, bf16[512,256]{1,0:T(8,128)(2,1)S(1)}, u32[]{:S(2)}, u32[]{:S(2)}) collective-permute-start(bf16[512,256]{1,0:T(8,128)(2,1)S(1)} %copy-done.15), channel_id=1, source_target_pairs={{0,2},{1,3},{2,0},{3,1},{4,6},{5,7},{6,4},{7,5},{8,10},{9,11},{10,... | collective-permute-start | bytes 786440 | tf_op jit(solution)/shard_map/ppermute | solution.py:359
  184.9 5.8 %copy-start.12 = (bf16[4,1,256,512]{3,2,1,0:T(8,128)(2,1)S(1)}, bf16[4,1,256,512]{3,2,1,0:T(8,128)(2,1)}, u32[]{:S(2)}) copy-start(bf16[4,1,256,512]{3,2,1,0:T(8,128)(2,1)} %get-tuple-element.11) | copy-start | bytes 3145732
  192.3 1.4 copy-start.14
